TPU v7x, 256 devices: a whole 4x4x8 slice. The times are simulated.
256 devices in a mesh: kv: 32 (over z, x), tp: 8 (over y, core).
Axes of the slice: x: 4, y: 4, z: 8, core: 2. Of those that a mesh axis runs over, the one named last changes fastest.
Arguments:
- tokens: bfloat16 [384, 2048], P('tp', 'kv'), may hold values from -10.5 to 10.5
- norm_gain: float32 [2048], P('kv'), may hold values from 0.1 to 1.9
- w_query: bfloat16 [2048, 2048], P('kv', 'tp'), may hold values from -0.125 to 0.125
- w_forget: bfloat16 [2048, 2048], P('kv', 'tp'), may hold values from -0.125 to 0.125
- w_input: bfloat16 [2048, 2048], P('kv', 'tp'), may hold values from -0.125 to 0.125
- w_gate: bfloat16 [2048, 2048], P('kv', 'tp'), may hold values from -0.125 to 0.125
- lower_bound: float32 [2048], P('tp'), may hold values from 0 to 0.9
- head_gain: float32 [16, 128], P('tp'), may hold values from 0.1 to 1.9
- recur_state: float32 [384, 16, 128, 128], P('kv', 'tp'), may hold values from -3 to 3
- w_out: bfloat16 [2048, 2048], P('tp', 'kv'), may hold values from -0.125 to 0.125
- mixer_gain: float32 [2048], P('kv'), may hold values from 0.1 to 1.9
- w_up: bfloat16 [2048, 8192], P('kv', 'tp'), may hold values from -0.125 to 0.125
- w_down: bfloat16 [8192, 2048], P('tp', 'kv'), may hold values from -0.0625 to 0.0625
Outputs:
- next_tokens: bfloat16 [384, 2048], P('tp', 'kv')
- next_state: float32 [384, 16, 128, 128], P('kv', 'tp')
All inputs are finite; a program needn't handle non-finite values.
Results may differ from a plain program's by a relative error of at most 0.03.
Values may be sent and summed in bfloat16 or wider, within the bound.
No kernel may reach another device: no remote copies, remote signals or barrier semaphores. Data moves between devices by JAX's collectives and lax.ppermute only.
A program may use at most 64 MiB of HBM per device.

v0:
```python
import math

import jax
import jax.numpy as jnp
from jax import lax
from jax.sharding import PartitionSpec as P

NORM_EPS = 1e-05


def laid_out(tiles, dim):
    tiles = jnp.moveaxis(tiles, 0, dim)
    dims = tiles.shape
    return tiles.reshape(*dims[:dim], dims[dim] * dims[dim + 1], *dims[dim + 2 :])


def from_everyone(value, axis):
    size = lax.axis_size(axis)
    return lax.all_to_all(
        jnp.broadcast_to(value[None], (size, *value.shape)), axis, 0, 0, tiled=True
    )


def gathered_copies(value, axis, dim):
    return laid_out(from_everyone(value, axis), dim)


def in_blocks(value, dim, size):
    dims = value.shape
    tiles = value.reshape(*dims[:dim], size, dims[dim] // size, *dims[dim + 1 :])
    return jnp.moveaxis(tiles, dim, 0)


def summed_on_arrival(value, axis, dim):
    tiles = in_blocks(value, dim, lax.axis_size(axis))
    arrived = lax.all_to_all(tiles, axis, split_axis=0, concat_axis=0, tiled=True)
    return arrived.astype(jnp.float32).sum(axis=0)


def taken_together(value, axis):
    return from_everyone(value, axis).sum(axis=0)


def in_one_piece(arrays, axis, dim, along):
    widths = [math.prod(a.shape[along:]) for a in arrays]
    both = jnp.concatenate(
        [a.reshape(*a.shape[:along], w) for a, w in zip(arrays, widths)], axis=along
    )
    result = summed_on_arrival(both, axis, dim)
    tiles = jnp.split(result, [sum(widths[:k]) for k in range(1, len(widths))], axis=along)
    return tuple(
        (b.reshape(*result.shape[:along], *a.shape[along:]) for a, b in zip(arrays, tiles))
    )


def project_in(row_block, norm_scale, weights, by_units):
    whole = gathered_copies(row_block, "tp", 0)
    tokens_f = whole.astype(jnp.float32)
    normed = (tokens_f * norm_scale).astype(jnp.bfloat16)
    squares = jnp.sum(tokens_f * tokens_f, axis=1)
    weight = jnp.concatenate(weights, axis=1)
    partial_value = jnp.dot(normed, weight, preferred_element_type=jnp.float32)
    width = normed.shape[1] * lax.axis_size("kv")
    if by_units:
        unit_cols = summed_on_arrival(partial_value.astype(jnp.bfloat16), "kv", 1)
        totals = taken_together(squares, "kv")
        return unit_cols * lax.rsqrt(totals / width + NORM_EPS)[:, None]
    owned, owned_sq = in_one_piece(
        (partial_value.astype(jnp.bfloat16), squares.astype(jnp.bfloat16)), "kv", 0, 1
    )
    row_scale = lax.rsqrt(owned_sq / width + NORM_EPS)
    return owned * row_scale[:, None]


def finish_out(partials):
    return summed_on_arrival(partials.astype(jnp.bfloat16), "tp", 0)


def project_out(values_bf, weight):
    product = jnp.dot(
        gathered_copies(values_bf, "kv", 0), weight, preferred_element_type=jnp.float32
    )
    partials = product.astype(jnp.bfloat16).astype(jnp.float32)
    return finish_out(partials)


def fold_out(values_bf, weight):
    summed = jnp.dot(
        gathered_copies(values_bf, "kv", 1), weight, preferred_element_type=jnp.float32
    )
    return finish_out(summed.astype(jnp.bfloat16).astype(jnp.float32))


def body(
    tokens,
    norm_gain,
    w_query,
    w_forget,
    w_input,
    w_gate,
    lower_bound,
    head_gain,
    recur_state,
    w_out,
    mixer_gain,
    w_up,
    w_down,
):
    projected = project_in(tokens, norm_gain, (w_query, w_forget, w_input, w_gate), False)
    rows_here = projected.shape[0]
    heads_here = recur_state.shape[1]
    key_size = recur_state.shape[2]
    val_size = recur_state.shape[3]
    span = heads_here * key_size
    val_span = heads_here * val_size
    queries = projected[:, :span].reshape(rows_here, heads_here, key_size)
    forget_raw = projected[:, span : 2 * span].reshape(rows_here, heads_here, key_size)
    values_in = projected[:, 2 * span : 2 * span + val_span].reshape(
        rows_here, heads_here, val_size
    )
    gate_raw = projected[:, 2 * span + val_span :]
    bound = lower_bound.reshape(heads_here, key_size)
    forget = bound + (1.0 - bound) * jax.nn.sigmoid(forget_raw)
    next_state = (
        forget[..., None] * recur_state + (1.0 - forget)[..., None] * values_in[:, :, None, :]
    )
    read_out = jnp.einsum("rhk,rhkv->rhv", queries, next_state, precision=lax.Precision.HIGHEST)
    read_out = (
        read_out
        * lax.rsqrt(jnp.mean(read_out * read_out, axis=2, keepdims=True) + NORM_EPS)
        * head_gain
    )
    mixture = (read_out.reshape(rows_here, val_span) * jax.nn.silu(gate_raw)).astype(jnp.bfloat16)
    mixed_rows = (tokens.astype(jnp.float32) + project_out(mixture, w_out)).astype(jnp.bfloat16)
    hidden_pre = project_in(mixed_rows, mixer_gain, (w_up,), True)
    hidden = jnp.square(jax.nn.relu(hidden_pre)).astype(jnp.bfloat16)
    down_out = fold_out(hidden, w_down)
    next_tokens = (mixed_rows.astype(jnp.float32) + down_out).astype(jnp.bfloat16)
    return (next_tokens, next_state)


def solution(mesh):
    in_specs = (
        P("tp", "kv"),
        P("kv"),
        P("kv", "tp"),
        P("kv", "tp"),
        P("kv", "tp"),
        P("kv", "tp"),
        P("tp"),
        P("tp", None),
        P("kv", "tp", None, None),
        P("tp", "kv"),
        P("kv"),
        P("kv", "tp"),
        P("tp", "kv"),
    )
    out_specs = (P("tp", "kv"), P("kv", "tp", None, None))
    return jax.shard_map(body, mesh=mesh, in_specs=in_specs, out_specs=out_specs, check_vma=False)
```

profile of v0, /device:TPU:1, one launch (start us, length us, event | category | flops | bytes accessed | tf_op | source)
XLA Modules:
  0.0 173.9 jit_solution(15843388054404118505)
XLA Ops:
  0.6 0.8 broadcast_in_dim.12
  1.4 0.1 reshape.139
  1.5 10.5 %all_to_all.46 = bf16[8,2,1536]{2,1,0:T(2,128)(2,1)S(1)} all-to-all(bf16[8,2,1536]{2,1,0:T(2,128)(2,1)S(1)} %reshape.139), channel_id=1, replica_groups=mesh['kv'=32,'tp'=8] {'tp'}, dimensions={0} | all-to-all | bytes 98304 | tf_op jit(solution)/shard_map/all_to_all | solution.py:19
  12.1 0.1 reshape.140
  12.2 0.1 multiply_reduce_fusion.1
  12.3 0.7 fusion.1
  13.0 0.2 convert_element_type.114
  13.2 1.1 convolution_convert_fusion.1
  14.4 0.2 concatenate.10
  14.6 1.2 pad_maximum_fusion
  15.7 11.2 %all-to-all-start.1 = ((bf16[32,12,1025]{2,1,0:T(8,128)(2,1)}), bf16[32,12,1025]{2,1,0:T(8,128)(2,1)S(1)}, u32[]{:S(2)}, u32[]{:S(2)}) async-start(bf16[32,12,1025]{2,1,0:T(8,128)(2,1)} %pad_maximum_fusion), calls=%async_computation.1 | async-start | bytes 2359296 | tf_op jit(solution)/shard_map/all_to_all | solution.py:36
  26.9 28.6 %all-to-all-done.1 = bf16[32,12,1025]{2,1,0:T(8,128)(2,1)S(1)} async-done(((bf16[32,12,1025]{2,1,0:T(8,128)(2,1)}), bf16[32,12,1025]{2,1,0:T(8,128)(2,1)S(1)}, u32[]{:S(2)}, u32[]{:S(2)}) %all-to-all-start.1) | async-done | bytes 787232 | tf_op jit(solution)/shard_map/all_to_all | solution.py:36
  55.5 0.2 convert_reduce_fusion
  55.7 0.1 fusion.14
  55.9 0.1 slice_multiply_fusion
  56.0 1.0 multiply_add_fusion
  57.1 1.4 fusion.16
  58.5 0.1 multiply_reduce_fusion.2
  58.6 0.1 multiply_multiply_fusion
  58.8 16.9 %all_to_all.47 = bf16[32,12,256]{2,1,0:T(8,128)(2,1)S(1)} all-to-all(bf16[32,12,256]{2,1,0:T(8,128)(2,1)S(1)} %broadcast_in_dim.13), channel_id=1, replica_groups=mesh['kv'=32,'tp'=8] {'kv'}, dimensions={0} | all-to-all | bytes 393216 | tf_op jit(solution)/shard_map/all_to_all | solution.py:19
  75.7 0.2 convolution_convert_fusion.3
  75.9 0.1 copy.62
  76.0 0.8 reshape.141
  76.8 7.0 %all-to-all-start.3 = ((bf16[8,2,1536]{2,1,0:T(2,128)(2,1)}), bf16[8,2,1536]{2,1,0:T(2,128)(2,1)S(1)}, u32[]{:S(2)}, u32[]{:S(2)}) async-start(bf16[8,2,1536]{2,1,0:T(2,128)(2,1)} %reshape.141), calls=%async_computation.3 | async-start | bytes 98304 | tf_op jit(solution)/shard_map/all_to_all | solution.py:36
  83.8 0.1 copy.50
  83.9 4.7 %all-to-all-done.3 = bf16[8,2,1536]{2,1,0:T(2,128)(2,1)S(1)} async-done(((bf16[8,2,1536]{2,1,0:T(2,128)(2,1)}), bf16[8,2,1536]{2,1,0:T(2,128)(2,1)S(1)}, u32[]{:S(2)}, u32[]{:S(2)}) %all-to-all-start.3) | async-done | bytes 49184 | tf_op jit(solution)/shard_map/all_to_all | solution.py:36
  88.6 0.1 reshape.142
  88.8 0.1 copy.54
  89.0 0.1 reshape.143
  89.1 7.9 %all_to_all.48 = bf16[8,2,1536]{2,1,0:T(2,128)(2,1)S(1)} all-to-all(bf16[8,2,1536]{2,1,0:T(2,128)(2,1)S(1)} %reshape.143), channel_id=1, replica_groups=mesh['kv'=32,'tp'=8] {'tp'}, dimensions={0} | all-to-all | bytes 98304 | tf_op jit(solution)/shard_map/all_to_all | solution.py:19
  97.0 0.1 reshape.144
  97.1 0.1 multiply_reduce_fusion
  97.3 0.1 broadcast_in_dim.15
  97.4 0.6 broadcast_in_dim.16
  98.0 3.8 %all-to-all-start.6 = ((f32[32,1,384]{2,1,0:T(1,128)}), f32[32,1,384]{2,1,0:T(1,128)S(1)}, u32[]{:S(2)}, u32[]{:S(2)}) async-start(f32[32,1,384]{2,1,0:T(1,128)} %broadcast_in_dim.16), calls=%async_computation.6 | async-start | bytes 98304 | tf_op jit(solution)/shard_map/all_to_all | solution.py:19
  101.9 0.3 convolution_convert_fusion
  102.2 1.2 copy.55
  103.4 7.3 %all-to-all-done.6 = f32[32,1,384]{2,1,0:T(1,128)S(1)} async-done(((f32[32,1,384]{2,1,0:T(1,128)}), f32[32,1,384]{2,1,0:T(1,128)S(1)}, u32[]{:S(2)}, u32[]{:S(2)}) %all-to-all-start.6) | async-done | bytes 49184 | tf_op jit(solution)/shard_map/all_to_all | solution.py:19
  110.7 3.9 %all-to-all-start.5 = ((bf16[32,384,32]{1,2,0:T(8,128)(2,1)}), bf16[32,384,32]{1,2,0:T(8,128)(2,1)S(1)}, u32[]{:S(2)}, u32[]{:S(2)}) async-start(bf16[32,384,32]{1,2,0:T(8,128)(2,1)} %bitcast.8), calls=%async_computation.5 | async-start | bytes 1572864 | tf_op jit(solution)/shard_map/all_to_all | solution.py:36
  114.7 20.5 %all-to-all-done.5 = bf16[32,384,32]{1,2,0:T(8,128)(2,1)S(1)} async-done(((bf16[32,384,32]{1,2,0:T(8,128)(2,1)}), bf16[32,384,32]{1,2,0:T(8,128)(2,1)S(1)}, u32[]{:S(2)}, u32[]{:S(2)}) %all-to-all-start.5) | async-done | bytes 786464 | tf_op jit(solution)/shard_map/all_to_all | solution.py:36
  135.2 0.1 convert_reduce_fusion.1
  135.4 25.8 %all_to_all.49 = bf16[32,384,32]{1,2,0:T(8,128)(2,1)S(1)} all-to-all(bf16[32,384,32]{1,2,0:T(8,128)(2,1)S(1)} %broadcast_in_dim.17), channel_id=1, replica_groups=mesh['kv'=32,'tp'=8] {'kv'}, dimensions={0} | all-to-all | bytes 1572864 | tf_op jit(solution)/shard_map/all_to_all | solution.py:19
  161.2 0.2 convolution_convert_fusion.2
  161.5 0.1 copy.63
  161.6 0.1 reshape.145
  161.8 11.2 %all_to_all.50 = bf16[8,2,1536]{2,1,0:T(2,128)(2,1)S(1)} all-to-all(bf16[8,2,1536]{2,1,0:T(2,128)(2,1)S(1)} %reshape.145), channel_id=1, replica_groups=mesh['kv'=32,'tp'=8] {'tp'}, dimensions={0} | all-to-all | bytes 98304 | tf_op jit(solution)/shard_map/all_to_all | solution.py:36
  173.0 0.1 reshape.146
  173.2 0.7 copy.59
  (42 shorter events, 0.7 us)
Async XLA Ops:
  0.6 101.2 %copy-start = (bf16[64,1024]{1,0:T(8,128)(2,1)S(1)}, bf16[64,1024]{1,0:T(8,128)(2,1)}, u32[]{:S(2)}) copy-start(bf16[64,1024]{1,0:T(8,128)(2,1)} %param.24) | copy-start | bytes 393220
  15.7 11.2 %copy-start.6 = (f32[256]{0:T(256)S(1)}, f32[256]{0:T(256)}, u32[]{:S(2)}) copy-start(f32[256]{0:T(256)} %param.19) | copy-start | bytes 3076
  15.7 40.3 %copy-start.2 = (f32[12,2,128,128]{3,2,1,0:T(8,128)S(1)}, f32[12,2,128,128]{3,2,1,0:T(8,128)}, u32[]{:S(2)}) copy-start(f32[12,2,128,128]{3,2,1,0:T(8,128)} %param.21) | copy-start | bytes 4718596
  15.7 39.8 %all-to-all-start.1 = ((bf16[32,12,1025]{2,1,0:T(8,128)(2,1)}), bf16[32,12,1025]{2,1,0:T(8,128)(2,1)S(1)}, u32[]{:S(2)}, u32[]{:S(2)}) async-start(bf16[32,12,1025]{2,1,0:T(8,128)(2,1)} %pad_maximum_fusion), calls=%async_computation.1 | async-start | bytes 2359296 | tf_op jit(solution)/shard_map/all_to_all | solution.py:36
  57.0 18.9 %copy-start.1 = (f32[12,2,128,128]{3,2,1,0:T(8,128)}, f32[12,2,128,128]{3,2,1,0:T(8,128)S(1)}, u32[]{:S(2)}) copy-start(f32[12,2,128,128]{3,2,1,0:T(8,128)S(1)} %multiply_add_fusion) | copy-start | bytes 4718596
  57.0 1.6 copy-start.7
  57.0 18.6 %copy-start.5 = (bf16[256,64]{0,1:T(8,128)(2,1)S(1)}, bf16[256,64]{0,1:T(8,128)(2,1)}, u32[]{:S(2)}) copy-start(bf16[256,64]{0,1:T(8,128)(2,1)} %param.22) | copy-start | bytes 98308
  57.1 26.7 %copy-start.4 = (bf16[48,64]{1,0:T(8,128)(2,1)S(1)}, bf16[48,64]{1,0:T(8,128)(2,1)}, u32[]{:S(2)}) copy-start(bf16[48,64]{1,0:T(8,128)(2,1)} %param.13) | copy-start | bytes 18436
  58.6 38.8 %copy-start.8 = (f32[64]{0:T(128)S(1)}, f32[64]{0:T(128)}, u32[]{:S(2)}) copy-start(f32[64]{0:T(128)} %param.23) | copy-start | bytes 772
  76.8 11.8 %all-to-all-start.3 = ((bf16[8,2,1536]{2,1,0:T(2,128)(2,1)}), bf16[8,2,1536]{2,1,0:T(2,128)(2,1)S(1)}, u32[]{:S(2)}, u32[]{:S(2)}) async-start(bf16[8,2,1536]{2,1,0:T(2,128)(2,1)} %reshape.141), calls=%async_computation.3 | async-start | bytes 98304 | tf_op jit(solution)/shard_map/all_to_all | solution.py:36
  98.0 12.7 %all-to-all-start.6 = ((f32[32,1,384]{2,1,0:T(1,128)}), f32[32,1,384]{2,1,0:T(1,128)S(1)}, u32[]{:S(2)}, u32[]{:S(2)}) async-start(f32[32,1,384]{2,1,0:T(1,128)} %broadcast_in_dim.16), calls=%async_computation.6 | async-start | bytes 98304 | tf_op jit(solution)/shard_map/all_to_all | solution.py:19
  110.7 24.5 %all-to-all-start.5 = ((bf16[32,384,32]{1,2,0:T(8,128)(2,1)}), bf16[32,384,32]{1,2,0:T(8,128)(2,1)S(1)}, u32[]{:S(2)}, u32[]{:S(2)}) async-start(bf16[32,384,32]{1,2,0:T(8,128)(2,1)} %bitcast.8), calls=%async_computation.5 | async-start | bytes 1572864 | tf_op jit(solution)/shard_map/all_to_all | solution.py:36
  114.7 46.5 %copy-start.3 = (bf16[1024,64]{0,1:T(8,128)(2,1)S(1)}, bf16[1024,64]{0,1:T(8,128)(2,1)}, u32[]{:S(2)}) copy-start(bf16[1024,64]{0,1:T(8,128)(2,1)} %param.25) | copy-start | bytes 393220
where the time goes:
time: 175 us; the launch traced here: 174 us
  blocking collectives  72.4 us (41%)
  waiting for transfers between devices  61.1 us (35%)
  starting transfers between devices  25.9 us (15%)
  local copies, waits for them, and re-layouts  6.19 us (4%)
  other arithmetic  4.01 us (2%)
  matrix products  3.34 us (2%)
    all_to_all x4, blocking collectives, from_everyone(): lax.all_to_all(jnp.broadcast_to(value[None], (size, *value.shape)), axis,...  61.1 us
    all_to_all x3, waiting for transfers between devices, summed_on_arrival(): lax.all_to_all(tiles, axis, split_axis=0, concat_axis=0, tiled=True)  53.8 us
    all_to_all x3, starting transfers between devices, summed_on_arrival(): lax.all_to_all(tiles, axis, split_axis=0, concat_axis=0, tiled=True)  22.1 us
    all_to_all x1, blocking collectives, summed_on_arrival(): lax.all_to_all(tiles, axis, split_axis=0, concat_axis=0, tiled=True)  11.2 us
    all_to_all x1, waiting for transfers between devices, from_everyone(): lax.all_to_all(jnp.broadcast_to(value[None], (size, *value.shape)), axis,...  7.32 us
    all_to_all x1, starting transfers between devices, from_everyone(): lax.all_to_all(jnp.broadcast_to(value[None], (size, *value.shape)), axis,...  3.84 us
  transfers between devices with their start and end apart: 4, of which 4 were waited for; matrix products, arithmetic and copies ran while one was open for 1% of the time, Pallas kernels for 0%

commit v1 on v0

v1 whole, which is shorter than its diff:
```python
import jax
import jax.numpy as jnp
from jax import lax
from jax.experimental import pallas as pl
from jax.experimental.pallas import tpu as pltpu
from jax.sharding import PartitionSpec as P

NORM_EPS = 1e-05
AXES = ("kv", "tp")
NZ, NX, NY, NC = 8, 4, 4, 2
BF, F32 = jnp.bfloat16, jnp.float32


def flat(z, x, y, c):
    return ((z * NX + x) * NY + y) * NC + c


def send(value, to):
    pairs = []
    for z in range(NZ):
        for x in range(NX):
            for y in range(NY):
                for c in range(NC):
                    pairs.append((flat(z, x, y, c), flat(*to(z, x, y, c))))
    return lax.ppermute(value, AXES, pairs)


def to_z(value, k):
    return send(value, lambda z, x, y, c: ((z + k) % NZ, x, y, c))


def to_x(value, k):
    return send(value, lambda z, x, y, c: (z, (x + k) % NX, y, c))


def to_y(value, k):
    return send(value, lambda z, x, y, c: (z, x, (y + k) % NY, c))


def to_core(value):
    return send(value, lambda z, x, y, c: (z, x, y, 1 - c))


def swap_rows(value):
    return send(value, lambda z, x, y, c: (NC * y + c, x, z // NC, z % NC))


def ring(shard, halves):
    got = [shard] + [None] * (NZ - 1)
    up, down = shard, shard
    for k in range(1, NZ // 2):
        up, down = to_z(up, 1), to_z(down, -1)
        got[NZ - k], got[k] = up, down
    first, second = halves
    a = to_z(up[first], 1)
    b = to_z(down[second], -1)
    got[NZ // 2] = (a, b)
    return got


def nt(a, b):
    return lax.dot_general(a, b, (((1,), (1,)), ((), ())), preferred_element_type=F32)


def nn(a, b):
    return jnp.dot(a, b, preferred_element_type=F32)


def lane_squares(v):
    s = v * v
    return (s[:, 0:128] + s[:, 128:256]) + (s[:, 256:384] + s[:, 384:512])


def call(kernel, outs, *args, scratch=()):
    in_specs = [
        pl.BlockSpec(memory_space=pltpu.SMEM if a.dtype == jnp.int32 else pltpu.VMEM) for a in args
    ]
    return pl.pallas_call(
        kernel,
        out_shape=outs,
        in_specs=in_specs,
        out_specs=jax.tree.map(lambda _: pl.BlockSpec(memory_space=pltpu.VMEM), outs),
        scratch_shapes=scratch,
    )(*args)


def project_kernel(tok_at, row_at, tok, w0, w1, w2, w3, w4a, w4b, w5, w6, w7, *rest):
    outs, acc = rest[:NX], rest[NX]
    xs = [tok[tok_at[k]] for k in range(NZ)]
    x_lo = jnp.concatenate(xs[:4], axis=1)
    x_hi = jnp.concatenate(xs[4:], axis=1)
    w_lo = jnp.concatenate([w[:, :1024] for w in (w0, w1, w2, w3)], axis=0)
    w_hi = jnp.concatenate([w[:, :1024] for w in (w4a, w4b, w5, w6, w7)], axis=0)
    main = nn(x_lo, w_lo) + nn(x_hi, w_hi)
    squares = lane_squares(jnp.concatenate([x_lo, x_hi], axis=1).astype(F32))
    for i in range(NX):
        acc[i, :, :1024] = main[12 * i : 12 * i + 12]
        acc[i, :, 1024:] = squares[12 * i : 12 * i + 12]
    for k in range(NX):
        outs[k][...] = acc[row_at[k]].astype(BF)


def attend_kernel(row_at, m0, m1, m2, m3, w0, w1, w2, w3, w4a, w4b, w5, w6, w7, out, acc):
    for k, m in enumerate((m0, m1, m2, m3)):
        acc[row_at[k]] = m[...].astype(F32)
    mix = jnp.concatenate([acc[i] for i in range(NX)], axis=0).astype(BF)
    w = jnp.concatenate([w[:, 1024:] for w in (w0, w1, w2, w3, w4a, w4b, w5, w6, w7)], axis=0)
    out[...] = nt(mix, w).astype(BF)


def up_kernel(tok_at, s0, s1, s2, s3, tok, w0, w1, w2, w3, w4, w5, w6, w7, mixed, msg):
    total = (s0[...].astype(F32) + s1[...].astype(F32)) + (s2[...].astype(F32) + s3[...].astype(F32))
    x = jnp.concatenate([tok[tok_at[k]] for k in range(NZ)], axis=1).astype(F32)
    rows = (x + total).astype(BF)
    mixed[...] = rows
    w = jnp.concatenate([w[:64, :] for w in (w0, w1, w2, w3, w4, w5, w6, w7)], axis=0)
    msg[:, :1024] = nn(rows, w).astype(BF)
    msg[:, 1024:] = lane_squares(rows.astype(F32)).astype(BF)


def down_kernel(put_at, h0, h1, h2, h3, w0, w1, w2, w3, w4, w5, w6, w7, out):
    total = (h0[...].astype(F32) + h1[...].astype(F32)) + (h2[...].astype(F32) + h3[...].astype(F32))
    scale = lax.rsqrt(jnp.sum(total[:, 1024:], axis=1, keepdims=True) / 2048 + NORM_EPS)
    hidden = jnp.square(jnp.maximum(total[:, :1024] * scale, 0.0)).astype(BF)
    ws = [w0[64:, :], w1[64:, :], w2[64:, :], w3[64:, :], w4[...], w5[64:, :], w6[64:, :], w7[64:, :]]
    part = nt(hidden, jnp.concatenate(ws, axis=0)).astype(BF)
    for k in range(NZ):
        out[put_at[k]] = part[:, 64 * k : 64 * (k + 1)]


def body(
    tokens, norm_gain, w_query, w_forget, w_input, w_gate, lower_bound, head_gain, recur_state,
    w_out, mixer_gain, w_up, w_down,
):
    kv, tp = lax.axis_index("kv"), lax.axis_index("tp")
    z, x, y, c = kv // NX, kv % NX, tp // NC, tp % NC
    kz = (z + jnp.arange(NZ)) % NZ
    tok_at = ((kz // NC - y) % NY * NC + (kz + c) % NC).astype(jnp.int32)
    put_at = ((kz + c) % NC * NY + (kz // NC - y) % NY).astype(jnp.int32)
    row_at = ((x + jnp.arange(NX)) % NX).astype(jnp.int32)

    w_in = jnp.concatenate([w_query, w_forget, w_input, w_gate], axis=1).astype(F32)
    early = jnp.concatenate([(w_in * norm_gain[:, None]).astype(BF), w_out.T], axis=1)
    late = jnp.concatenate([(w_up.astype(F32) * mixer_gain[:, None]).astype(BF), w_down.T], axis=0)

    mine = swap_rows(tokens)
    pair = jnp.stack([mine, to_core(mine)])
    tok = jnp.concatenate([pair] + [to_y(pair, -j) for j in range(1, NY)], axis=0)

    e = ring(early, (slice(0, 32), slice(32, 64)))
    ea, eb = e[4]
    ew = (*e[:4], ea, eb, *e[5:])
    parts = call(
        project_kernel,
        [jax.ShapeDtypeStruct((12, 1152), BF)] * NX,
        tok_at, row_at, tok, *ew,
        scratch=[pltpu.VMEM((NX, 12, 1152), F32)],
    )
    total = parts[0].astype(F32)
    for k in range(1, NX):
        total = total + to_x(parts[k], k).astype(F32)
    scale = lax.rsqrt(jnp.sum(total[:, 1024:], axis=1) / 2048 + NORM_EPS)
    projected = total[:, :1024] * scale[:, None]

    queries = projected[:, :256].reshape(12, 2, 128)
    forget_raw = projected[:, 256:512].reshape(12, 2, 128)
    values_in = projected[:, 512:768].reshape(12, 2, 128)
    gate_raw = projected[:, 768:]
    bound = lower_bound.reshape(2, 128)
    forget = bound + (1.0 - bound) * jax.nn.sigmoid(forget_raw)
    next_state = (
        forget[..., None] * recur_state + (1.0 - forget)[..., None] * values_in[:, :, None, :]
    )
    read_out = jnp.einsum("rhk,rhkv->rhv", queries, next_state, precision=lax.Precision.HIGHEST)
    read_out = (
        read_out
        * lax.rsqrt(jnp.mean(read_out * read_out, axis=2, keepdims=True) + NORM_EPS)
        * head_gain
    )
    mixture = (read_out.reshape(12, 256) * jax.nn.silu(gate_raw)).astype(BF)

    mixes = [mixture] + [to_x(mixture, -k) for k in range(1, NX)]
    attn = call(
        attend_kernel,
        jax.ShapeDtypeStruct((48, 512), BF),
        row_at, *mixes, *ew,
        scratch=[pltpu.VMEM((NX, 12, 256), F32)],
    )
    duo = (attn.astype(F32) + to_core(attn).astype(F32)).astype(BF)
    sums = [duo] + [to_y(duo, k) for k in range(1, NY)]

    f = ring(late, (slice(0, 64), slice(64, 128)))
    up4, down4 = f[4]
    mixed, msg = call(
        up_kernel,
        [jax.ShapeDtypeStruct((48, 512), BF), jax.ShapeDtypeStruct((48, 1152), BF)],
        tok_at, *sums, tok, *f[:4], up4, *f[5:],
    )
    msgs = [msg] + [to_x(msg, k) for k in range(1, NX)]
    blocks = call(
        down_kernel,
        jax.ShapeDtypeStruct((NZ, 48, 64), BF),
        put_at, *msgs, *f[:4], down4, *f[5:],
    )
    kept = (blocks[:NY].astype(F32) + to_core(blocks[NY:]).astype(F32)).astype(BF)
    down_out = kept[0].astype(F32)
    for k in range(1, NY):
        down_out = down_out + to_y(kept[k], k).astype(F32)
    own = lax.dynamic_slice_in_dim(mixed, (tp - z) % NZ * 64, 64, 1)
    next_tokens = swap_rows((own.astype(F32) + down_out).astype(BF))
    return (next_tokens, next_state)


def solution(mesh):
    in_specs = (
        P("tp", "kv"),
        P("kv"),
        P("kv", "tp"),
        P("kv", "tp"),
        P("kv", "tp"),
        P("kv", "tp"),
        P("tp"),
        P("tp", None),
        P("kv", "tp", None, None),
        P("tp", "kv"),
        P("kv"),
        P("kv", "tp"),
        P("tp", "kv"),
    )
    out_specs = (P("tp", "kv"), P("kv", "tp", None, None))
    return jax.shard_map(body, mesh=mesh, in_specs=in_specs, out_specs=out_specs, check_vma=False)
```

time: 175 us -> 129 us (0.74)
  the two profiles are of different devices: /device:TPU:1 before, /device:TPU:16 now
where the time goes in v1:
time: 129 us; the launch traced here: 128 us
  starting transfers between devices  61.3 us (48%)
  waiting for transfers between devices  37 us (29%)
  other arithmetic  11 us (9%)
  Pallas kernels  10.1 us (8%)
  local copies, waits for them, and re-layouts  5.97 us (5%)
  matrix products  1.41 us (1%)
    ppermute x39, starting transfers between devices, send(): return lax.ppermute(value, AXES, pairs)  61.3 us
    ppermute x39, waiting for transfers between devices, send(): return lax.ppermute(value, AXES, pairs)  37 us
    pallas_call x4, Pallas kernels, call(): pl.pallas_call(kernel, out_shape=outs, in_specs=in_specs, out_specs=jax.t...  10.1 us
    unnamed x73, local copies, waits for them, and re-layouts  5.08 us
  transfers between devices with their start and end apart: 39, of which 15 were waited for; matrix products, arithmetic and copies ran while one was open for 7% of the time, Pallas kernels for 6%

profile of v1, /device:TPU:16, one launch (start us, length us, event | category | flops | bytes accessed | tf_op | source)
XLA Modules:
  0.0 127.9 jit_solution(18341199893189851599)
XLA Ops:
  0.6 0.9 multiply_convert_fusion.1
  2.3 2.0 %collective-permute-start.8 = (bf16[64,1280]{1,0:T(8,128)(2,1)S(1)}, bf16[64,1280]{1,0:T(8,128)(2,1)S(1)}, u32[]{:S(2)}, u32[]{:S(2)}) collective-permute-start(bf16[64,1280]{1,0:T(8,128)(2,1)S(1)} %pad_maximum_fusion.1.w0), channel_id=1, source_target_pairs={{0,32},{1,33},{2,34},{3,35},{4,36},{5,37},{6,38},{7,39},{8,40},{9,... | collective-permute-start | bytes 491528 | tf_op jit(solution)/shard_map/ppermute | solution.py:25
  4.3 4.0 %collective-permute-start.5 = (bf16[64,1280]{1,0:T(8,128)(2,1)S(1)}, bf16[64,1280]{1,0:T(8,128)(2,1)S(1)}, u32[]{:S(2)}, u32[]{:S(2)}) collective-permute-start(bf16[64,1280]{1,0:T(8,128)(2,1)S(1)} %pad_maximum_fusion.1.w0), channel_id=1, source_target_pairs={{0,224},{1,225},{2,226},{3,227},{4,228},{5,229},{6,230},{7,231},{8... | collective-permute-start | bytes 491528 | tf_op jit(solution)/shard_map/ppermute | solution.py:25
  8.4 1.0 multiply_convert_fusion
  9.4 0.9 pad_maximum_fusion.w0
  10.4 3.2 %collective-permute-start.23 = (bf16[128,1024]{1,0:T(8,128)(2,1)S(1)}, bf16[128,1024]{1,0:T(8,128)(2,1)S(1)}, u32[]{:S(2)}, u32[]{:S(2)}) collective-permute-start(bf16[128,1024]{1,0:T(8,128)(2,1)S(1)} %pad_maximum_fusion.w0), channel_id=1, source_target_pairs={{0,224},{1,225},{2,226},{3,227},{4,228},{5,229},{6,230},{7,231},{8... | collective-permute-start | bytes 786440 | tf_op jit(solution)/shard_map/ppermute | solution.py:25
  13.6 6.2 %collective-permute-start = (bf16[48,64]{1,0:T(8,128)(2,1)}, bf16[48,64]{1,0:T(8,128)(2,1)S(1)}, u32[]{:S(2)}, u32[]{:S(2)}) collective-permute-start(bf16[48,64]{1,0:T(8,128)(2,1)} %param.13), channel_id=1, source_target_pairs={{0,0},{1,32},{2,64},{3,96},{4,128},{5,160},{6,192},{7,224},{8,8},{... | collective-permute-start | bytes 18440 | tf_op jit(solution)/shard_map/ppermute | solution.py:25
  20.9 4.8 %collective-permute-done = bf16[48,64]{1,0:T(8,128)(2,1)S(1)} collective-permute-done((bf16[48,64]{1,0:T(8,128)(2,1)}, bf16[48,64]{1,0:T(8,128)(2,1)S(1)}, u32[]{:S(2)}, u32[]{:S(2)}) %collective-permute-start) | collective-permute-done | bytes 6176 | tf_op jit(solution)/shard_map/ppermute | solution.py:25
  25.7 1.2 collective-permute-done.1
  27.1 3.2 %collective-permute-start.6 = (bf16[64,1280]{1,0:T(8,128)(2,1)S(1)}, bf16[64,1280]{1,0:T(8,128)(2,1)S(1)}, u32[]{:S(2)}, u32[]{:S(2)}) collective-permute-start(bf16[64,1280]{1,0:T(8,128)(2,1)S(1)} %collective-permute-done.5.w1), channel_id=1, source_target_pairs={{0,224},{1,225},{2,226},{3,227},{4,228},{5,229},{6,230},{7,231},{8... | collective-permute-start | bytes 491528 | tf_op jit(solution)/shard_map/ppermute | solution.py:25
  31.5 3.1 %collective-permute-done.9.w6 = bf16[64,1280]{1,0:T(8,128)(2,1)S(1)} collective-permute-done((bf16[64,1280]{1,0:T(8,128)(2,1)S(1)}, bf16[64,1280]{1,0:T(8,128)(2,1)S(1)}, u32[]{:S(2)}, u32[]{:S(2)}) %collective-permute-start.9) | collective-permute-done | bytes 163872 | tf_op jit(solution)/shard_map/ppermute | solution.py:25
  34.6 3.2 %collective-permute-start.7 = (bf16[64,1280]{1,0:T(8,128)(2,1)S(1)}, bf16[64,1280]{1,0:T(8,128)(2,1)S(1)}, u32[]{:S(2)}, u32[]{:S(2)}) collective-permute-start(bf16[64,1280]{1,0:T(8,128)(2,1)S(1)} %collective-permute-done.6.w2), channel_id=1, source_target_pairs={{0,224},{1,225},{2,226},{3,227},{4,228},{5,229},{6,230},{7,231},{8... | collective-permute-start | bytes 491528 | tf_op jit(solution)/shard_map/ppermute | solution.py:25
  37.8 1.7 %collective-permute-start.4 = (bf16[2,48,64]{2,1,0:T(8,128)(2,1)S(1)}, bf16[2,48,64]{2,1,0:T(8,128)(2,1)S(1)}, u32[]{:S(2)}, u32[]{:S(2)}) collective-permute-start(bf16[2,48,64]{2,1,0:T(8,128)(2,1)S(1)} %pad_maximum_fusion.2), channel_id=1, source_target_pairs={{0,2},{1,3},{2,4},{3,5},{4,6},{5,7},{6,0},{7,1},{8,10},{9,11},{10,... | collective-permute-start | bytes 36872 | tf_op jit(solution)/shard_map/ppermute | solution.py:25
  39.7 1.5 %collective-permute-done.10.w5 = bf16[64,1280]{1,0:T(8,128)(2,1)S(1)} collective-permute-done((bf16[64,1280]{1,0:T(8,128)(2,1)S(1)}, bf16[64,1280]{1,0:T(8,128)(2,1)S(1)}, u32[]{:S(2)}, u32[]{:S(2)}) %collective-permute-start.10) | collective-permute-done | bytes 163872 | tf_op jit(solution)/shard_map/ppermute | solution.py:25
  41.3 3.3 %collective-permute-start.12 = (bf16[32,1280]{1,0:T(8,128)(2,1)S(1)}, bf16[32,1280]{1,0:T(8,128)(2,1)S(1)}, u32[]{:S(2)}, u32[]{:S(2)}) collective-permute-start(bf16[32,1280]{1,0:T(8,128)(2,1)S(1)} %slice.65), channel_id=1, source_target_pairs={{0,224},{1,225},{2,226},{3,227},{4,228},{5,229},{6,230},{7,231},{8... | collective-permute-start | bytes 245768 | tf_op jit(solution)/shard_map/ppermute | solution.py:25
  44.6 4.4 %collective-permute-done.11.w4a = bf16[32,1280]{1,0:T(8,128)(2,1)S(1)} collective-permute-done((bf16[32,1280]{1,0:T(8,128)(2,1)S(1)}, bf16[32,1280]{1,0:T(8,128)(2,1)S(1)}, u32[]{:S(2)}, u32[]{:S(2)}) %collective-permute-start.11) | collective-permute-done | bytes 81952 | tf_op jit(solution)/shard_map/ppermute | solution.py:25
  50.3 2.4 %shard_map.140 = (bf16[12,1152]{1,0:T(8,128)(2,1)}, bf16[12,1152]{1,0:T(8,128)(2,1)}, bf16[12,1152]{1,0:T(8,128)(2,1)}, bf16[12,1152]{1,0:T(8,128)(2,1)}) custom-call(s32[8]{0:T(128)} %multiply_add_fusion.3.tok_at, s32[4]{0:T(128)} %and_select_fusion.row_at, bf16[8,48,64]{2,1,0:T(8,128)(2,1)} %copy-done.15, bf16[64,1280]{1,0:T(8,128)(2,1)} %copy-done.4, ...), custom_call_target="tpu_custom_call" | custom-call | tf_op jit(solution)/shard_map/pallas_call | solution.py:78
  52.7 1.6 %collective-permute-start.13 = (bf16[12,1152]{1,0:T(8,128)(2,1)}, bf16[12,1152]{1,0:T(8,128)(2,1)S(1)}, u32[]{:S(2)}, u32[]{:S(2)}) collective-permute-start(bf16[12,1152]{1,0:T(8,128)(2,1)} %get-tuple-element.9), channel_id=1, source_target_pairs={{0,8},{1,9},{2,10},{3,11},{4,12},{5,13},{6,14},{7,15},{8,16},{9,17... | collective-permute-start | bytes 82952 | tf_op jit(solution)/shard_map/ppermute | solution.py:25
  54.2 2.7 %collective-permute-start.14 = (bf16[12,1152]{1,0:T(8,128)(2,1)}, bf16[12,1152]{1,0:T(8,128)(2,1)S(1)}, u32[]{:S(2)}, u32[]{:S(2)}) collective-permute-start(bf16[12,1152]{1,0:T(8,128)(2,1)} %get-tuple-element.10), channel_id=1, source_target_pairs={{0,16},{1,17},{2,18},{3,19},{4,20},{5,21},{6,22},{7,23},{8,24},{9,... | collective-permute-start | bytes 82952 | tf_op jit(solution)/shard_map/ppermute | solution.py:25
  57.0 1.4 %collective-permute-start.15 = (bf16[12,1152]{1,0:T(8,128)(2,1)}, bf16[12,1152]{1,0:T(8,128)(2,1)S(1)}, u32[]{:S(2)}, u32[]{:S(2)}) collective-permute-start(bf16[12,1152]{1,0:T(8,128)(2,1)} %get-tuple-element.11), channel_id=1, source_target_pairs={{0,24},{1,25},{2,26},{3,27},{4,28},{5,29},{6,30},{7,31},{8,0},{9,1... | collective-permute-start | bytes 82952 | tf_op jit(solution)/shard_map/ppermute | solution.py:25
  59.2 1.3 %collective-permute-start.28 = (bf16[128,1024]{1,0:T(8,128)(2,1)S(1)}, bf16[128,1024]{1,0:T(8,128)(2,1)S(1)}, u32[]{:S(2)}, u32[]{:S(2)}) collective-permute-start(bf16[128,1024]{1,0:T(8,128)(2,1)S(1)} %collective-permute-done.27.w6), channel_id=1, source_target_pairs={{0,32},{1,33},{2,34},{3,35},{4,36},{5,37},{6,38},{7,39},{8,40},{9,... | collective-permute-start | bytes 786440 | tf_op jit(solution)/shard_map/ppermute | solution.py:25
  61.1 0.8 convert_add_fusion
  62.2 2.1 %multiply_add_fusion = f32[12,2,128,128]{3,2,1,0:T(8,128)S(1)} fusion(f32[12,2,128,128]{3,2,1,0:T(8,128)} %param.21, f32[12,2,128]{2,1,0:T(2,128)S(1)} %mul.107, f32[12,2,128]{2,1,0:T(2,128)S(1)} %get-tuple-element.14, f32[12,2,128]{2,1,0:T(2,128)S(1)} %get-tuple-element.15), kind=kLoop, calls=%fused_computation | loop fusion | flops 1179648 | bytes 3182592 | tf_op jit(solution)/shard_map/add | solution.py:172
  64.4 1.4 %fusion.11 = f32[12,2,1,128]{3,2,1,0:T(1,128)S(1)} fusion(f32[12,2,128,1]{2,3,1,0:T(1,128)S(1)} %bitcast.32, f32[12,2,128,128]{3,2,1,0:T(8,128)S(1)} %multiply_add_fusion), kind=kOutput, calls=%fused_computation.59 | convolution fusion | flops 4718592 | bytes 1597440 | tf_op jit(solution)/shard_map/rhk,rhkv->rhv/dot_general | solution.py:174
  66.1 2.7 %collective-permute-start.16 = (bf16[12,256]{1,0:T(8,128)(2,1)S(1)}, bf16[12,256]{1,0:T(8,128)(2,1)S(1)}, u32[]{:S(2)}, u32[]{:S(2)}) collective-permute-start(bf16[12,256]{1,0:T(8,128)(2,1)S(1)} %multiply_convert_fusion.2.m0), channel_id=1, source_target_pairs={{0,24},{1,25},{2,26},{3,27},{4,28},{5,29},{6,30},{7,31},{8,0},{9,1... | collective-permute-start | bytes 18440 | tf_op jit(solution)/shard_map/ppermute | solution.py:25
  68.8 1.0 collective-permute-start.18
  70.2 3.8 %collective-permute-done.17.m2 = bf16[12,256]{1,0:T(8,128)(2,1)S(1)} collective-permute-done((bf16[12,256]{1,0:T(8,128)(2,1)S(1)}, bf16[12,256]{1,0:T(8,128)(2,1)S(1)}, u32[]{:S(2)}, u32[]{:S(2)}) %collective-permute-start.17) | collective-permute-done | bytes 6176 | tf_op jit(solution)/shard_map/ppermute | solution.py:25
  75.2 2.2 %shard_map.141 = bf16[48,512]{1,0:T(8,128)(2,1)} custom-call(s32[4]{0:T(128)} %and_select_fusion.row_at, bf16[12,256]{1,0:T(8,128)(2,1)} %copy-done.27, bf16[12,256]{1,0:T(8,128)(2,1)} %copy-done.28, bf16[12,256]{1,0:T(8,128)(2,1)} %copy-done.29, bf16[12,256]{1,0:T(8,128)(2,1)} %copy-done.30, bf16[64,1280]{1,0:T(8,128)(2,1)} %copy-done.4, ...), custom_call_target="tpu_custom_call" | custom-call | tf_op jit(solution)/shard_map/pallas_call | solution.py:78
  78.2 1.4 %collective-permute-start.29 = (bf16[64,1024]{1,0:T(8,128)(2,1)S(1)}, bf16[64,1024]{1,0:T(8,128)(2,1)S(1)}, u32[]{:S(2)}, u32[]{:S(2)}) collective-permute-start(bf16[64,1024]{1,0:T(8,128)(2,1)S(1)} %slice.72), channel_id=1, source_target_pairs={{0,32},{1,33},{2,34},{3,35},{4,36},{5,37},{6,38},{7,39},{8,40},{9,... | collective-permute-start | bytes 393224 | tf_op jit(solution)/shard_map/ppermute | solution.py:25
  79.6 0.8 add_convert_fusion.1.s0
  80.5 1.2 collective-permute-start.20
  81.7 1.0 collective-permute-start.21
  82.7 0.8 collective-permute-start.22
  83.5 2.6 %collective-permute-done.25.w3 = bf16[128,1024]{1,0:T(8,128)(2,1)S(1)} collective-permute-done((bf16[128,1024]{1,0:T(8,128)(2,1)S(1)}, bf16[128,1024]{1,0:T(8,128)(2,1)S(1)}, u32[]{:S(2)}, u32[]{:S(2)}) %collective-permute-start.25) | collective-permute-done | bytes 262176 | tf_op jit(solution)/shard_map/ppermute | solution.py:25
  86.2 2.0 %collective-permute-start.33 = (bf16[64,1024]{1,0:T(8,128)(2,1)S(1)}, bf16[64,1024]{1,0:T(8,128)(2,1)S(1)}, u32[]{:S(2)}, u32[]{:S(2)}) collective-permute-start(bf16[64,1024]{1,0:T(8,128)(2,1)S(1)} %slice.73), channel_id=1, source_target_pairs={{0,224},{1,225},{2,226},{3,227},{4,228},{5,229},{6,230},{7,231},{8... | collective-permute-start | bytes 393224 | tf_op jit(solution)/shard_map/ppermute | solution.py:25
  89.4 2.6 %shard_map.142 = (bf16[48,512]{1,0:T(8,128)(2,1)}, bf16[48,1152]{1,0:T(8,128)(2,1)}) custom-call(s32[8]{0:T(128)} %multiply_add_fusion.3.tok_at, bf16[48,512]{1,0:T(8,128)(2,1)} %copy-done.18, bf16[48,512]{1,0:T(8,128)(2,1)} %copy-done.24, bf16[48,512]{1,0:T(8,128)(2,1)} %copy-done.25, bf16[48,512]{1,0:T(8,128)(2,1)} %copy-done.26, ...), custom_call_target="tpu_custom_call" | custom-call | tf_op jit(solution)/shard_map/pallas_call | solution.py:78
  92.0 2.0 %collective-permute-start.31 = (bf16[48,1152]{1,0:T(8,128)(2,1)}, bf16[48,1152]{1,0:T(8,128)(2,1)S(1)}, u32[]{:S(2)}, u32[]{:S(2)}) collective-permute-start(bf16[48,1152]{1,0:T(8,128)(2,1)} %get-tuple-element.13.h0), channel_id=1, source_target_pairs={{0,16},{1,17},{2,18},{3,19},{4,20},{5,21},{6,22},{7,23},{8,24},{9,... | collective-permute-start | bytes 331784 | tf_op jit(solution)/shard_map/ppermute | solution.py:25
  94.1 2.0 %collective-permute-start.32 = (bf16[48,1152]{1,0:T(8,128)(2,1)}, bf16[48,1152]{1,0:T(8,128)(2,1)S(1)}, u32[]{:S(2)}, u32[]{:S(2)}) collective-permute-start(bf16[48,1152]{1,0:T(8,128)(2,1)} %get-tuple-element.13.h0), channel_id=1, source_target_pairs={{0,24},{1,25},{2,26},{3,27},{4,28},{5,29},{6,30},{7,31},{8,0},{9,1... | collective-permute-start | bytes 331784 | tf_op jit(solution)/shard_map/ppermute | solution.py:25
  96.6 3.4 %collective-permute-done.30.h1 = bf16[48,1152]{1,0:T(8,128)(2,1)S(1)} collective-permute-done((bf16[48,1152]{1,0:T(8,128)(2,1)}, bf16[48,1152]{1,0:T(8,128)(2,1)S(1)}, u32[]{:S(2)}, u32[]{:S(2)}) %collective-permute-start.30) | collective-permute-done | bytes 110624 | tf_op jit(solution)/shard_map/ppermute | solution.py:25
  101.4 2.8 %shard_map.143 = bf16[8,48,64]{2,1,0:T(8,128)(2,1)} custom-call(s32[8]{0:T(128)} %multiply_add_fusion.2.put_at, bf16[48,1152]{1,0:T(8,128)(2,1)} %get-tuple-element.13.h0, bf16[48,1152]{1,0:T(8,128)(2,1)} %copy-done.21, bf16[48,1152]{1,0:T(8,128)(2,1)} %copy-done.22, bf16[48,1152]{1,0:T(8,128)(2,1)} %copy-done.23, bf16[128,1024]{1,0:T(8,128)(2,1)} %copy-done.1, ...), custom_call_target="tpu_custom_call" | custom-call | tf_op jit(solution)/shard_map/pallas_call | solution.py:78
  104.2 0.8 slice.75
  105.0 1.2 collective-permute-done.34
  106.3 0.8 add_convert_fusion
  107.1 2.3 %collective-permute-start.35 = (bf16[48,64]{1,0:T(8,128)(2,1)S(1)}, bf16[48,64]{1,0:T(8,128)(2,1)S(1)}, u32[]{:S(2)}, u32[]{:S(2)}) collective-permute-start(bf16[48,64]{1,0:T(8,128)(2,1)S(1)} %get-tuple-element.19), channel_id=1, source_target_pairs={{0,2},{1,3},{2,4},{3,5},{4,6},{5,7},{6,0},{7,1},{8,10},{9,11},{10,... | collective-permute-start | bytes 18440 | tf_op jit(solution)/shard_map/ppermute | solution.py:25
  109.4 2.0 %collective-permute-start.37 = (bf16[48,64]{1,0:T(8,128)(2,1)S(1)}, bf16[48,64]{1,0:T(8,128)(2,1)S(1)}, u32[]{:S(2)}, u32[]{:S(2)}) collective-permute-start(bf16[48,64]{1,0:T(8,128)(2,1)S(1)} %get-tuple-element.20), channel_id=1, source_target_pairs={{0,6},{1,7},{2,0},{3,1},{4,2},{5,3},{6,4},{7,5},{8,14},{9,15},{10,... | collective-permute-start | bytes 18440 | tf_op jit(solution)/shard_map/ppermute | solution.py:25
  111.4 3.2 %collective-permute-done.36 = bf16[48,64]{1,0:T(8,128)(2,1)S(1)} collective-permute-done((bf16[48,64]{1,0:T(8,128)(2,1)S(1)}, bf16[48,64]{1,0:T(8,128)(2,1)S(1)}, u32[]{:S(2)}, u32[]{:S(2)}) %collective-permute-start.36) | collective-permute-done | bytes 6176 | tf_op jit(solution)/shard_map/ppermute | solution.py:25
  115.4 6.2 %collective-permute-start.38 = (bf16[48,64]{1,0:T(8,128)(2,1)S(1)}, bf16[48,64]{1,0:T(8,128)(2,1)S(1)}, u32[]{:S(2)}, u32[]{:S(2)}) collective-permute-start(bf16[48,64]{1,0:T(8,128)(2,1)S(1)} %fusion.3), channel_id=1, source_target_pairs={{0,0},{1,32},{2,64},{3,96},{4,128},{5,160},{6,192},{7,224},{8,8},{... | collective-permute-start | bytes 18440 | tf_op jit(solution)/shard_map/ppermute | solution.py:25
  121.7 5.6 %collective-permute-done.38 = bf16[48,64]{1,0:T(8,128)(2,1)S(1)} collective-permute-done((bf16[48,64]{1,0:T(8,128)(2,1)S(1)}, bf16[48,64]{1,0:T(8,128)(2,1)S(1)}, u32[]{:S(2)}, u32[]{:S(2)}) %collective-permute-start.38) | collective-permute-done | bytes 6176 | tf_op jit(solution)/shard_map/ppermute | solution.py:25
  (141 shorter events, 13.6 us)
Async XLA Ops:
  1.5 56.9 %copy-start.31 = (f32[256]{0:T(256)S(1)}, f32[256]{0:T(256)}, u32[]{:S(2)}) copy-start(f32[256]{0:T(256)} %param.19) | copy-start | bytes 3076
  2.3 46.7 %copy-start.4 = (bf16[64,1280]{1,0:T(8,128)(2,1)}, bf16[64,1280]{1,0:T(8,128)(2,1)S(1)}, u32[]{:S(2)}) copy-start(bf16[64,1280]{1,0:T(8,128)(2,1)S(1)} %pad_maximum_fusion.1.w0) | copy-start | bytes 491524
  2.3 24.7 %collective-permute-start.8 = (bf16[64,1280]{1,0:T(8,128)(2,1)S(1)}, bf16[64,1280]{1,0:T(8,128)(2,1)S(1)}, u32[]{:S(2)}, u32[]{:S(2)}) collective-permute-start(bf16[64,1280]{1,0:T(8,128)(2,1)S(1)} %pad_maximum_fusion.1.w0), channel_id=1, source_target_pairs={{0,32},{1,33},{2,34},{3,35},{4,36},{5,37},{6,38},{7,39},{8,40},{9,... | collective-permute-start | bytes 491528 | tf_op jit(solution)/shard_map/ppermute | solution.py:25
  4.3 22.8 %collective-permute-start.5 = (bf16[64,1280]{1,0:T(8,128)(2,1)S(1)}, bf16[64,1280]{1,0:T(8,128)(2,1)S(1)}, u32[]{:S(2)}, u32[]{:S(2)}) collective-permute-start(bf16[64,1280]{1,0:T(8,128)(2,1)S(1)} %pad_maximum_fusion.1.w0), channel_id=1, source_target_pairs={{0,224},{1,225},{2,226},{3,227},{4,228},{5,229},{6,230},{7,231},{8... | collective-permute-start | bytes 491528 | tf_op jit(solution)/shard_map/ppermute | solution.py:25
  10.3 54.1 %copy-start.1 = (bf16[128,1024]{1,0:T(8,128)(2,1)}, bf16[128,1024]{1,0:T(8,128)(2,1)S(1)}, u32[]{:S(2)}) copy-start(bf16[128,1024]{1,0:T(8,128)(2,1)S(1)} %pad_maximum_fusion.w0) | copy-start | bytes 786436
  10.3 29.3 %collective-permute-start.26 = (bf16[128,1024]{1,0:T(8,128)(2,1)S(1)}, bf16[128,1024]{1,0:T(8,128)(2,1)S(1)}, u32[]{:S(2)}, u32[]{:S(2)}) collective-permute-start(bf16[128,1024]{1,0:T(8,128)(2,1)S(1)} %pad_maximum_fusion.w0), channel_id=1, source_target_pairs={{0,32},{1,33},{2,34},{3,35},{4,36},{5,37},{6,38},{7,39},{8,40},{9,... | collective-permute-start | bytes 786440 | tf_op jit(solution)/shard_map/ppermute | solution.py:25
  10.4 48.0 %collective-permute-start.23 = (bf16[128,1024]{1,0:T(8,128)(2,1)S(1)}, bf16[128,1024]{1,0:T(8,128)(2,1)S(1)}, u32[]{:S(2)}, u32[]{:S(2)}) collective-permute-start(bf16[128,1024]{1,0:T(8,128)(2,1)S(1)} %pad_maximum_fusion.w0), channel_id=1, source_target_pairs={{0,224},{1,225},{2,226},{3,227},{4,228},{5,229},{6,230},{7,231},{8... | collective-permute-start | bytes 786440 | tf_op jit(solution)/shard_map/ppermute | solution.py:25
  13.6 12.1 %collective-permute-start = (bf16[48,64]{1,0:T(8,128)(2,1)}, bf16[48,64]{1,0:T(8,128)(2,1)S(1)}, u32[]{:S(2)}, u32[]{:S(2)}) collective-permute-start(bf16[48,64]{1,0:T(8,128)(2,1)} %param.13), channel_id=1, source_target_pairs={{0,0},{1,32},{2,64},{3,96},{4,128},{5,160},{6,192},{7,224},{8,8},{... | collective-permute-start | bytes 18440 | tf_op jit(solution)/shard_map/ppermute | solution.py:25
  25.7 1.2 collective-permute-start.1
  26.9 3.9 %collective-permute-start.2 = (bf16[2,48,64]{2,1,0:T(8,128)(2,1)S(1)}, bf16[2,48,64]{2,1,0:T(8,128)(2,1)S(1)}, u32[]{:S(2)}, u32[]{:S(2)}) collective-permute-start(bf16[2,48,64]{2,1,0:T(8,128)(2,1)S(1)} %pad_maximum_fusion.2), channel_id=1, source_target_pairs={{0,6},{1,7},{2,0},{3,1},{4,2},{5,3},{6,4},{7,5},{8,14},{9,15},{10,... | collective-permute-start | bytes 36872 | tf_op jit(solution)/shard_map/ppermute | solution.py:25
  27.0 22.0 %copy-start.11 = (bf16[64,1280]{1,0:T(8,128)(2,1)}, bf16[64,1280]{1,0:T(8,128)(2,1)S(1)}, u32[]{:S(2)}) copy-start(bf16[64,1280]{1,0:T(8,128)(2,1)S(1)} %collective-permute-done.8.w7) | copy-start | bytes 491524
  27.0 7.6 %collective-permute-start.9 = (bf16[64,1280]{1,0:T(8,128)(2,1)S(1)}, bf16[64,1280]{1,0:T(8,128)(2,1)S(1)}, u32[]{:S(2)}, u32[]{:S(2)}) collective-permute-start(bf16[64,1280]{1,0:T(8,128)(2,1)S(1)} %collective-permute-done.8.w7), channel_id=1, source_target_pairs={{0,32},{1,33},{2,34},{3,35},{4,36},{5,37},{6,38},{7,39},{8,40},{9,... | collective-permute-start | bytes 491528 | tf_op jit(solution)/shard_map/ppermute | solution.py:25
  27.1 21.9 %copy-start.12 = (bf16[64,1280]{1,0:T(8,128)(2,1)}, bf16[64,1280]{1,0:T(8,128)(2,1)S(1)}, u32[]{:S(2)}) copy-start(bf16[64,1280]{1,0:T(8,128)(2,1)S(1)} %collective-permute-done.5.w1) | copy-start | bytes 491524
  27.1 7.5 %collective-permute-start.6 = (bf16[64,1280]{1,0:T(8,128)(2,1)S(1)}, bf16[64,1280]{1,0:T(8,128)(2,1)S(1)}, u32[]{:S(2)}, u32[]{:S(2)}) collective-permute-start(bf16[64,1280]{1,0:T(8,128)(2,1)S(1)} %collective-permute-done.5.w1), channel_id=1, source_target_pairs={{0,224},{1,225},{2,226},{3,227},{4,228},{5,229},{6,230},{7,231},{8... | collective-permute-start | bytes 491528 | tf_op jit(solution)/shard_map/ppermute | solution.py:25
  30.8 7.0 %collective-permute-start.3 = (bf16[2,48,64]{2,1,0:T(8,128)(2,1)S(1)}, bf16[2,48,64]{2,1,0:T(8,128)(2,1)S(1)}, u32[]{:S(2)}, u32[]{:S(2)}) collective-permute-start(bf16[2,48,64]{2,1,0:T(8,128)(2,1)S(1)} %pad_maximum_fusion.2), channel_id=1, source_target_pairs={{0,4},{1,5},{2,6},{3,7},{4,0},{5,1},{6,2},{7,3},{8,12},{9,13},{10,... | collective-permute-start | bytes 36872 | tf_op jit(solution)/shard_map/ppermute | solution.py:25
  34.6 14.5 %copy-start.13 = (bf16[64,1280]{1,0:T(8,128)(2,1)}, bf16[64,1280]{1,0:T(8,128)(2,1)S(1)}, u32[]{:S(2)}) copy-start(bf16[64,1280]{1,0:T(8,128)(2,1)S(1)} %collective-permute-done.9.w6) | copy-start | bytes 491524
  34.6 6.6 %collective-permute-start.10 = (bf16[64,1280]{1,0:T(8,128)(2,1)S(1)}, bf16[64,1280]{1,0:T(8,128)(2,1)S(1)}, u32[]{:S(2)}, u32[]{:S(2)}) collective-permute-start(bf16[64,1280]{1,0:T(8,128)(2,1)S(1)} %collective-permute-done.9.w6), channel_id=1, source_target_pairs={{0,32},{1,33},{2,34},{3,35},{4,36},{5,37},{6,38},{7,39},{8,40},{9,... | collective-permute-start | bytes 491528 | tf_op jit(solution)/shard_map/ppermute | solution.py:25
  34.6 14.5 %copy-start.14 = (bf16[64,1280]{1,0:T(8,128)(2,1)}, bf16[64,1280]{1,0:T(8,128)(2,1)S(1)}, u32[]{:S(2)}) copy-start(bf16[64,1280]{1,0:T(8,128)(2,1)S(1)} %collective-permute-done.6.w2) | copy-start | bytes 491524
  34.6 6.7 %collective-permute-start.7 = (bf16[64,1280]{1,0:T(8,128)(2,1)S(1)}, bf16[64,1280]{1,0:T(8,128)(2,1)S(1)}, u32[]{:S(2)}, u32[]{:S(2)}) collective-permute-start(bf16[64,1280]{1,0:T(8,128)(2,1)S(1)} %collective-permute-done.6.w2), channel_id=1, source_target_pairs={{0,224},{1,225},{2,226},{3,227},{4,228},{5,229},{6,230},{7,231},{8... | collective-permute-start | bytes 491528 | tf_op jit(solution)/shard_map/ppermute | solution.py:25
  37.8 6.8 %collective-permute-start.4 = (bf16[2,48,64]{2,1,0:T(8,128)(2,1)S(1)}, bf16[2,48,64]{2,1,0:T(8,128)(2,1)S(1)}, u32[]{:S(2)}, u32[]{:S(2)}) collective-permute-start(bf16[2,48,64]{2,1,0:T(8,128)(2,1)S(1)} %pad_maximum_fusion.2), channel_id=1, source_target_pairs={{0,2},{1,3},{2,4},{3,5},{4,6},{5,7},{6,0},{7,1},{8,10},{9,11},{10,... | collective-permute-start | bytes 36872 | tf_op jit(solution)/shard_map/ppermute | solution.py:25
  39.6 24.8 %copy-start.5 = (bf16[128,1024]{1,0:T(8,128)(2,1)}, bf16[128,1024]{1,0:T(8,128)(2,1)S(1)}, u32[]{:S(2)}) copy-start(bf16[128,1024]{1,0:T(8,128)(2,1)S(1)} %collective-permute-done.26.w7) | copy-start | bytes 786436
  39.6 19.6 %collective-permute-start.27 = (bf16[128,1024]{1,0:T(8,128)(2,1)S(1)}, bf16[128,1024]{1,0:T(8,128)(2,1)S(1)}, u32[]{:S(2)}, u32[]{:S(2)}) collective-permute-start(bf16[128,1024]{1,0:T(8,128)(2,1)S(1)} %collective-permute-done.26.w7), channel_id=1, source_target_pairs={{0,32},{1,33},{2,34},{3,35},{4,36},{5,37},{6,38},{7,39},{8,40},{9,... | collective-permute-start | bytes 786440 | tf_op jit(solution)/shard_map/ppermute | solution.py:25
  41.2 7.8 %collective-permute-start.11 = (bf16[32,1280]{1,0:T(8,128)(2,1)S(1)}, bf16[32,1280]{1,0:T(8,128)(2,1)S(1)}, u32[]{:S(2)}, u32[]{:S(2)}) collective-permute-start(bf16[32,1280]{1,0:T(8,128)(2,1)S(1)} %slice.64), channel_id=1, source_target_pairs={{0,32},{1,33},{2,34},{3,35},{4,36},{5,37},{6,38},{7,39},{8,40},{9,... | collective-permute-start | bytes 245768 | tf_op jit(solution)/shard_map/ppermute | solution.py:25
  41.3 7.7 %collective-permute-start.12 = (bf16[32,1280]{1,0:T(8,128)(2,1)S(1)}, bf16[32,1280]{1,0:T(8,128)(2,1)S(1)}, u32[]{:S(2)}, u32[]{:S(2)}) collective-permute-start(bf16[32,1280]{1,0:T(8,128)(2,1)S(1)} %slice.65), channel_id=1, source_target_pairs={{0,224},{1,225},{2,226},{3,227},{4,228},{5,229},{6,230},{7,231},{8... | collective-permute-start | bytes 245768 | tf_op jit(solution)/shard_map/ppermute | solution.py:25
  52.7 7.9 %collective-permute-start.13 = (bf16[12,1152]{1,0:T(8,128)(2,1)}, bf16[12,1152]{1,0:T(8,128)(2,1)S(1)}, u32[]{:S(2)}, u32[]{:S(2)}) collective-permute-start(bf16[12,1152]{1,0:T(8,128)(2,1)} %get-tuple-element.9), channel_id=1, source_target_pairs={{0,8},{1,9},{2,10},{3,11},{4,12},{5,13},{6,14},{7,15},{8,16},{9,17... | collective-permute-start | bytes 82952 | tf_op jit(solution)/shard_map/ppermute | solution.py:25
  54.2 6.3 %collective-permute-start.14 = (bf16[12,1152]{1,0:T(8,128)(2,1)}, bf16[12,1152]{1,0:T(8,128)(2,1)S(1)}, u32[]{:S(2)}, u32[]{:S(2)}) collective-permute-start(bf16[12,1152]{1,0:T(8,128)(2,1)} %get-tuple-element.10), channel_id=1, source_target_pairs={{0,16},{1,17},{2,18},{3,19},{4,20},{5,21},{6,22},{7,23},{8,24},{9,... | collective-permute-start | bytes 82952 | tf_op jit(solution)/shard_map/ppermute | solution.py:25
  57.0 4.2 %collective-permute-start.15 = (bf16[12,1152]{1,0:T(8,128)(2,1)}, bf16[12,1152]{1,0:T(8,128)(2,1)S(1)}, u32[]{:S(2)}, u32[]{:S(2)}) collective-permute-start(bf16[12,1152]{1,0:T(8,128)(2,1)} %get-tuple-element.11), channel_id=1, source_target_pairs={{0,24},{1,25},{2,26},{3,27},{4,28},{5,29},{6,30},{7,31},{8,0},{9,1... | collective-permute-start | bytes 82952 | tf_op jit(solution)/shard_map/ppermute | solution.py:25
  58.4 19.0 %collective-permute-start.24 = (bf16[128,1024]{1,0:T(8,128)(2,1)S(1)}, bf16[128,1024]{1,0:T(8,128)(2,1)S(1)}, u32[]{:S(2)}, u32[]{:S(2)}) collective-permute-start(bf16[128,1024]{1,0:T(8,128)(2,1)S(1)} %collective-permute-done.23.w1), channel_id=1, source_target_pairs={{0,224},{1,225},{2,226},{3,227},{4,228},{5,229},{6,230},{7,231},{8... | collective-permute-start | bytes 786440 | tf_op jit(solution)/shard_map/ppermute | solution.py:25
  59.2 19.0 %collective-permute-start.28 = (bf16[128,1024]{1,0:T(8,128)(2,1)S(1)}, bf16[128,1024]{1,0:T(8,128)(2,1)S(1)}, u32[]{:S(2)}, u32[]{:S(2)}) collective-permute-start(bf16[128,1024]{1,0:T(8,128)(2,1)S(1)} %collective-permute-done.27.w6), channel_id=1, source_target_pairs={{0,32},{1,33},{2,34},{3,35},{4,36},{5,37},{6,38},{7,39},{8,40},{9,... | collective-permute-start | bytes 786440 | tf_op jit(solution)/shard_map/ppermute | solution.py:25
  64.4 13.0 %copy-start = (f32[12,2,128,128]{3,2,1,0:T(8,128)}, f32[12,2,128,128]{3,2,1,0:T(8,128)S(1)}, u32[]{:S(2)}) copy-start(f32[12,2,128,128]{3,2,1,0:T(8,128)S(1)} %multiply_add_fusion) | copy-start | bytes 4718596
  66.1 4.1 %collective-permute-start.16 = (bf16[12,256]{1,0:T(8,128)(2,1)S(1)}, bf16[12,256]{1,0:T(8,128)(2,1)S(1)}, u32[]{:S(2)}, u32[]{:S(2)}) collective-permute-start(bf16[12,256]{1,0:T(8,128)(2,1)S(1)} %multiply_convert_fusion.2.m0), channel_id=1, source_target_pairs={{0,24},{1,25},{2,26},{3,27},{4,28},{5,29},{6,30},{7,31},{8,0},{9,1... | collective-permute-start | bytes 18440 | tf_op jit(solution)/shard_map/ppermute | solution.py:25
  68.8 5.2 %collective-permute-start.17 = (bf16[12,256]{1,0:T(8,128)(2,1)S(1)}, bf16[12,256]{1,0:T(8,128)(2,1)S(1)}, u32[]{:S(2)}, u32[]{:S(2)}) collective-permute-start(bf16[12,256]{1,0:T(8,128)(2,1)S(1)} %multiply_convert_fusion.2.m0), channel_id=1, source_target_pairs={{0,16},{1,17},{2,18},{3,19},{4,20},{5,21},{6,22},{7,23},{8,24},{9,... | collective-permute-start | bytes 18440 | tf_op jit(solution)/shard_map/ppermute | solution.py:25
  68.8 5.2 %collective-permute-start.18 = (bf16[12,256]{1,0:T(8,128)(2,1)S(1)}, bf16[12,256]{1,0:T(8,128)(2,1)S(1)}, u32[]{:S(2)}, u32[]{:S(2)}) collective-permute-start(bf16[12,256]{1,0:T(8,128)(2,1)S(1)} %multiply_convert_fusion.2.m0), channel_id=1, source_target_pairs={{0,8},{1,9},{2,10},{3,11},{4,12},{5,13},{6,14},{7,15},{8,16},{9,17... | collective-permute-start | bytes 18440 | tf_op jit(solution)/shard_map/ppermute | solution.py:25
  77.4 2.2 %collective-permute-start.19 = (bf16[48,512]{1,0:T(8,128)(2,1)}, bf16[48,512]{1,0:T(8,128)(2,1)S(1)}, u32[]{:S(2)}, u32[]{:S(2)}) collective-permute-start(bf16[48,512]{1,0:T(8,128)(2,1)} %shard_map.141), channel_id=1, source_target_pairs={{0,1},{1,0},{2,3},{3,2},{4,5},{5,4},{6,7},{7,6},{8,9},{9,8},{10,11... | collective-permute-start | bytes 147464 | tf_op jit(solution)/shard_map/ppermute | solution.py:25
  77.4 8.7 %collective-permute-start.25 = (bf16[128,1024]{1,0:T(8,128)(2,1)S(1)}, bf16[128,1024]{1,0:T(8,128)(2,1)S(1)}, u32[]{:S(2)}, u32[]{:S(2)}) collective-permute-start(bf16[128,1024]{1,0:T(8,128)(2,1)S(1)} %collective-permute-done.24.w2), channel_id=1, source_target_pairs={{0,224},{1,225},{2,226},{3,227},{4,228},{5,229},{6,230},{7,231},{8... | collective-permute-start | bytes 786440 | tf_op jit(solution)/shard_map/ppermute | solution.py:25
  78.2 9.9 %collective-permute-start.29 = (bf16[64,1024]{1,0:T(8,128)(2,1)S(1)}, bf16[64,1024]{1,0:T(8,128)(2,1)S(1)}, u32[]{:S(2)}, u32[]{:S(2)}) collective-permute-start(bf16[64,1024]{1,0:T(8,128)(2,1)S(1)} %slice.72), channel_id=1, source_target_pairs={{0,32},{1,33},{2,34},{3,35},{4,36},{5,37},{6,38},{7,39},{8,40},{9,... | collective-permute-start | bytes 393224 | tf_op jit(solution)/shard_map/ppermute | solution.py:25
  80.5 7.7 %collective-permute-start.20 = (bf16[48,512]{1,0:T(8,128)(2,1)S(1)}, bf16[48,512]{1,0:T(8,128)(2,1)S(1)}, u32[]{:S(2)}, u32[]{:S(2)}) collective-permute-start(bf16[48,512]{1,0:T(8,128)(2,1)S(1)} %add_convert_fusion.1.s0), channel_id=1, source_target_pairs={{0,2},{1,3},{2,4},{3,5},{4,6},{5,7},{6,0},{7,1},{8,10},{9,11},{10,... | collective-permute-start | bytes 147464 | tf_op jit(solution)/shard_map/ppermute | solution.py:25
  81.7 6.5 %collective-permute-start.21 = (bf16[48,512]{1,0:T(8,128)(2,1)S(1)}, bf16[48,512]{1,0:T(8,128)(2,1)S(1)}, u32[]{:S(2)}, u32[]{:S(2)}) collective-permute-start(bf16[48,512]{1,0:T(8,128)(2,1)S(1)} %add_convert_fusion.1.s0), channel_id=1, source_target_pairs={{0,4},{1,5},{2,6},{3,7},{4,0},{5,1},{6,2},{7,3},{8,12},{9,13},{10,... | collective-permute-start | bytes 147464 | tf_op jit(solution)/shard_map/ppermute | solution.py:25
  82.7 5.5 %collective-permute-start.22 = (bf16[48,512]{1,0:T(8,128)(2,1)S(1)}, bf16[48,512]{1,0:T(8,128)(2,1)S(1)}, u32[]{:S(2)}, u32[]{:S(2)}) collective-permute-start(bf16[48,512]{1,0:T(8,128)(2,1)S(1)} %add_convert_fusion.1.s0), channel_id=1, source_target_pairs={{0,6},{1,7},{2,0},{3,1},{4,2},{5,3},{6,4},{7,5},{8,14},{9,15},{10,... | collective-permute-start | bytes 147464 | tf_op jit(solution)/shard_map/ppermute | solution.py:25
  86.2 10.5 %collective-permute-start.33 = (bf16[64,1024]{1,0:T(8,128)(2,1)S(1)}, bf16[64,1024]{1,0:T(8,128)(2,1)S(1)}, u32[]{:S(2)}, u32[]{:S(2)}) collective-permute-start(bf16[64,1024]{1,0:T(8,128)(2,1)S(1)} %slice.73), channel_id=1, source_target_pairs={{0,224},{1,225},{2,226},{3,227},{4,228},{5,229},{6,230},{7,231},{8... | collective-permute-start | bytes 393224 | tf_op jit(solution)/shard_map/ppermute | solution.py:25
  92.0 8.0 %collective-permute-start.30 = (bf16[48,1152]{1,0:T(8,128)(2,1)}, bf16[48,1152]{1,0:T(8,128)(2,1)S(1)}, u32[]{:S(2)}, u32[]{:S(2)}) collective-permute-start(bf16[48,1152]{1,0:T(8,128)(2,1)} %get-tuple-element.13.h0), channel_id=1, source_target_pairs={{0,8},{1,9},{2,10},{3,11},{4,12},{5,13},{6,14},{7,15},{8,16},{9,17... | collective-permute-start | bytes 331784 | tf_op jit(solution)/shard_map/ppermute | solution.py:25
  92.0 8.0 %collective-permute-start.31 = (bf16[48,1152]{1,0:T(8,128)(2,1)}, bf16[48,1152]{1,0:T(8,128)(2,1)S(1)}, u32[]{:S(2)}, u32[]{:S(2)}) collective-permute-start(bf16[48,1152]{1,0:T(8,128)(2,1)} %get-tuple-element.13.h0), channel_id=1, source_target_pairs={{0,16},{1,17},{2,18},{3,19},{4,20},{5,21},{6,22},{7,23},{8,24},{9,... | collective-permute-start | bytes 331784 | tf_op jit(solution)/shard_map/ppermute | solution.py:25
  94.1 6.6 %collective-permute-start.32 = (bf16[48,1152]{1,0:T(8,128)(2,1)}, bf16[48,1152]{1,0:T(8,128)(2,1)S(1)}, u32[]{:S(2)}, u32[]{:S(2)}) collective-permute-start(bf16[48,1152]{1,0:T(8,128)(2,1)} %get-tuple-element.13.h0), channel_id=1, source_target_pairs={{0,24},{1,25},{2,26},{3,27},{4,28},{5,29},{6,30},{7,31},{8,0},{9,1... | collective-permute-start | bytes 331784 | tf_op jit(solution)/shard_map/ppermute | solution.py:25
  105.0 1.2 collective-permute-start.34
  107.1 4.3 %collective-permute-start.35 = (bf16[48,64]{1,0:T(8,128)(2,1)S(1)}, bf16[48,64]{1,0:T(8,128)(2,1)S(1)}, u32[]{:S(2)}, u32[]{:S(2)}) collective-permute-start(bf16[48,64]{1,0:T(8,128)(2,1)S(1)} %get-tuple-element.19), channel_id=1, source_target_pairs={{0,2},{1,3},{2,4},{3,5},{4,6},{5,7},{6,0},{7,1},{8,10},{9,11},{10,... | collective-permute-start | bytes 18440 | tf_op jit(solution)/shard_map/ppermute | solution.py:25
  109.4 5.2 %collective-permute-start.36 = (bf16[48,64]{1,0:T(8,128)(2,1)S(1)}, bf16[48,64]{1,0:T(8,128)(2,1)S(1)}, u32[]{:S(2)}, u32[]{:S(2)}) collective-permute-start(bf16[48,64]{1,0:T(8,128)(2,1)S(1)} %get-tuple-element.21), channel_id=1, source_target_pairs={{0,4},{1,5},{2,6},{3,7},{4,0},{5,1},{6,2},{7,3},{8,12},{9,13},{10,... | collective-permute-start | bytes 18440 | tf_op jit(solution)/shard_map/ppermute | solution.py:25
  109.4 5.2 %collective-permute-start.37 = (bf16[48,64]{1,0:T(8,128)(2,1)S(1)}, bf16[48,64]{1,0:T(8,128)(2,1)S(1)}, u32[]{:S(2)}, u32[]{:S(2)}) collective-permute-start(bf16[48,64]{1,0:T(8,128)(2,1)S(1)} %get-tuple-element.20), channel_id=1, source_target_pairs={{0,6},{1,7},{2,0},{3,1},{4,2},{5,3},{6,4},{7,5},{8,14},{9,15},{10,... | collective-permute-start | bytes 18440 | tf_op jit(solution)/shard_map/ppermute | solution.py:25
  115.4 11.9 %collective-permute-start.38 = (bf16[48,64]{1,0:T(8,128)(2,1)S(1)}, bf16[48,64]{1,0:T(8,128)(2,1)S(1)}, u32[]{:S(2)}, u32[]{:S(2)}) collective-permute-start(bf16[48,64]{1,0:T(8,128)(2,1)S(1)} %fusion.3), channel_id=1, source_target_pairs={{0,0},{1,32},{2,64},{3,96},{4,128},{5,160},{6,192},{7,224},{8,8},{... | collective-permute-start | bytes 18440 | tf_op jit(solution)/shard_map/ppermute | solution.py:25
  (24 other events, 86.0 us)

commit v2 on v1

v2 whole, which is shorter than its diff:
```python
import jax
import jax.numpy as jnp
from jax import lax
from jax.experimental import pallas as pl
from jax.experimental.pallas import tpu as pltpu
from jax.sharding import Mesh, PartitionSpec as P

NORM_EPS = 1e-05
NZ, NX, NY, NC = 8, 4, 4, 2
NT = NY * NC
AXES = ("z", "x", "y", "core")
TP = ("y", "core")
XTP = ("x", "y", "core")
BF, F32 = jnp.bfloat16, jnp.float32


def flat(z, x, y, c):
    return ((z * NX + x) * NY + y) * NC + c


def send(value, to):
    pairs = []
    for z in range(NZ):
        for x in range(NX):
            for y in range(NY):
                for c in range(NC):
                    pairs.append((flat(z, x, y, c), flat(*to(z, x, y, c))))
    return lax.ppermute(value, AXES, pairs)


def to_x(value, k):
    return send(value, lambda z, x, y, c: (z, (x + k) % NX, y, c))


def swap_rows(value):
    return send(value, lambda z, x, y, c: (NC * y + c, x, z // NC, z % NC))


def exchange(tiles, axis):
    return lax.all_to_all(tiles, axis, 0, 0, tiled=True)


def gathered(value, axis):
    size = lax.axis_size(axis)
    return exchange(jnp.broadcast_to(value[None], (size, *value.shape)), axis)


def after(value, *others):
    return lax.optimization_barrier((value, *others))[0]


def nt(a, b, precision=None):
    return lax.dot_general(
        a, b, (((1,), (1,)), ((), ())), preferred_element_type=F32, precision=precision
    )


def with_squares(main, rows):
    n = main.shape[0] // 16
    sums = nt(jnp.ones((8, rows.shape[1]), F32), rows * rows, lax.Precision.HIGHEST)[:1]
    if n * 16 < 128:
        sums = jnp.concatenate([sums, jnp.zeros((1, 128 - n * 16), F32)], axis=1)
    high = sums.astype(BF).astype(F32)
    low = sums - high
    row = lax.broadcasted_iota(jnp.int32, (n, 16, 128), 1)
    cube = main.reshape(n, 16, 1024)
    head = jnp.where(row == 12, high[None], jnp.where(row == 13, low[None], cube[:, :, :128]))
    return jnp.concatenate([head, cube[:, :, 128:]], axis=2).astype(BF)


def scaled(total, place):
    sums = total[12:13, :128] + total[13:14, :128]
    row = lax.broadcasted_iota(jnp.int32, (16, 128), 0)
    lane = lax.broadcasted_iota(jnp.int32, (16, 128), 1)
    mine = jnp.where((lane == row + 16 * place) & (row < 12), sums, 0.0)
    square = jnp.sum(mine, axis=1, keepdims=True)
    return total * lax.rsqrt(square / 2048 + NORM_EPS)


def call(kernel, outs, *args, scratch=()):
    in_specs = [
        pl.BlockSpec(memory_space=pltpu.SMEM if a.dtype == jnp.int32 else pltpu.VMEM) for a in args
    ]
    return pl.pallas_call(
        kernel,
        out_shape=outs,
        in_specs=in_specs,
        out_specs=jax.tree.map(lambda _: pl.BlockSpec(memory_space=pltpu.VMEM), outs),
        scratch_shapes=scratch,
    )(*args)


def shape(*dims, dtype=BF):
    return jax.ShapeDtypeStruct(dims, dtype)


def project_kernel(tok, w, out):
    x = jnp.concatenate([tok[i].reshape(128, 64) for i in range(NX)], axis=1)
    main = jnp.dot(x, w[...].reshape(256, 1024), preferred_element_type=F32)
    out[...] = with_squares(main, x.astype(F32))


def recur_kernel(place, msg, state, bound, gain, mixture, new):
    total = msg[0].astype(F32)
    for k in range(1, NZ):
        total = total + msg[k].astype(F32)
    total = scaled(total, place[0])
    reads = [[], []]
    for h in range(2):
        at = slice(128 * h, 128 * h + 128)
        low = bound[:, at]
        forget = low + (1.0 - low) * jax.nn.sigmoid(total[:, 256:512][:, at])
        f_t = forget.T
        q_t = total[:, :256][:, at].T
        v = total[:, 512:768][:, at]
        for r in range(12):
            row = v[r : r + 1]
            s = row + f_t[:, r : r + 1] * (state[r, h] - row)
            new[r, h] = s
            reads[h].append(jnp.sum(q_t[:, r : r + 1] * s, axis=0, keepdims=True))
    for h in range(2):
        at = slice(128 * h, 128 * h + 128)
        read = jnp.concatenate(reads[h] + [jnp.zeros((4, 128), F32)], axis=0)
        read = read * lax.rsqrt(jnp.mean(read * read, axis=1, keepdims=True) + NORM_EPS)
        mixture[:, at] = (read * gain[h : h + 1] * jax.nn.silu(total[:, 768:][:, at])).astype(BF)


def attend_kernel(row_at, m0, m1, m2, m3, w, tok, out, acc):
    for k, m in enumerate((m0, m1, m2, m3)):
        acc[row_at[k]] = m[...]
    part = nt(acc[...].reshape(64, 256), w[...].reshape(512, 256))
    part = jnp.concatenate([part[16 * i : 16 * i + 12] for i in range(NX)], axis=0)
    part = (part + tok[...].astype(F32)).astype(BF)
    for k in range(NT):
        out[k] = part


def up_kernel(row_at, parts, w, mixed, o0, o1, o2, o3, acc):
    total = parts[0].astype(F32)
    for k in range(1, NT):
        total = total + parts[k].astype(F32)
    rows = total.astype(BF)
    mixed[...] = rows
    wide = rows.astype(F32)
    pad = jnp.zeros((4, 512), F32)
    pieces = [p for i in range(NX) for p in (wide[12 * i : 12 * i + 12], pad)]
    wide = jnp.concatenate(pieces, axis=0)
    main = jnp.dot(wide.astype(BF), w[...].reshape(512, 1024), preferred_element_type=F32)
    acc[...] = with_squares(main, wide)
    for k, o in enumerate((o0, o1, o2, o3)):
        o[...] = acc[row_at[k]]


def hidden_kernel(place, m0, m1, m2, m3, out):
    total = (m0[...].astype(F32) + m1[...].astype(F32)) + (m2[...].astype(F32) + m3[...].astype(F32))
    row = lax.broadcasted_iota(jnp.int32, (16, 1024), 0)
    pre = jnp.where(row < 12, scaled(total, place[0]), 0.0)
    hidden = jnp.square(jnp.maximum(pre, 0.0)).astype(BF)
    for k in range(NZ):
        out[k] = hidden


def down_kernel(hidden, w, out):
    part = nt(hidden[...].reshape(128, 1024), w[...].reshape(256, 1024)).astype(BF)
    for i in range(NX):
        out[i] = part[:, 64 * i : 64 * i + 64].reshape(NZ, 16, 64)


def last_kernel(parts, mixed, out):
    for i in range(NX):
        total = parts[i, 0].astype(F32)
        for k in range(1, NT):
            total = total + parts[i, k].astype(F32)
        out[12 * i : 12 * i + 12, :] = total[:12] + mixed[12 * i : 12 * i + 12, :].astype(F32)


def body(
    tokens, norm_gain, w_query, w_forget, w_input, w_gate, lower_bound, head_gain, recur_state,
    w_out, mixer_gain, w_up, w_down,
):
    z, x = lax.axis_index("z"), lax.axis_index("x")
    t = lax.axis_index(TP)
    row_at = ((x + jnp.arange(NX)) % NX).astype(jnp.int32)
    z_at, x_at = z.reshape(1).astype(jnp.int32), x.reshape(1).astype(jnp.int32)

    cut = jnp.pad(tokens.reshape(NX, 1, 12, 64), ((0, 0), (0, 0), (0, 4), (0, 0)))
    cut = jnp.broadcast_to(cut, (NX, NT, 16, 64)).reshape(NX * NT, 16, 64)
    tok = exchange(cut, XTP).reshape(NX, NT, 16, 64)
    w_in = jnp.concatenate([w_query, w_forget, w_input, w_gate], axis=1).astype(F32)
    w_in = gathered((w_in * norm_gain[:, None]).astype(BF), "x")
    moved = swap_rows(tokens)
    w_out = gathered(w_out.T, "z")

    parts = call(project_kernel, shape(NZ, 16, 1024), tok, w_in)
    w_down = gathered(after(w_down.T, parts), "x")
    msg = exchange(parts, "z")
    w_up = (w_up.astype(F32) * mixer_gain[:, None]).astype(BF)
    w_up = gathered(after(w_up, msg), "z")
    mixture, next_state = call(
        recur_kernel,
        [shape(16, 256), shape(12, 2, 128, 128, dtype=F32)],
        z_at, msg, recur_state, lower_bound.reshape(1, 256), head_gain,
    )

    mixes = [mixture] + [to_x(mixture, -k) for k in range(1, NX)]
    block = lax.broadcasted_iota(jnp.int32, (48, 512), 1) // 64
    spread = jnp.where(block == t, jnp.tile(moved, (1, NZ)), jnp.zeros((), BF))
    attn = call(
        attend_kernel,
        shape(NT, 48, 512),
        row_at, *mixes, w_out, spread,
        scratch=[pltpu.VMEM((NX, 16, 256), BF)],
    )
    mixed, *outs = call(
        up_kernel,
        [shape(48, 512)] + [shape(16, 1024)] * NX,
        row_at, exchange(attn, TP), w_up,
        scratch=[pltpu.VMEM((NX, 16, 1024), BF)],
    )
    ups = [outs[0]] + [to_x(outs[k], k) for k in range(1, NX)]
    home = swap_rows(lax.dynamic_slice_in_dim(mixed, t * 64, 64, 1))
    hidden = exchange(call(hidden_kernel, shape(NZ, 16, 1024), x_at, *ups), "z")
    downs = call(down_kernel, shape(NX, NT, 16, 64), hidden, w_down)
    back = exchange(downs.reshape(NX * NT, 16, 64), XTP).reshape(NX, NT, 16, 64)
    last = call(last_kernel, shape(48, 64, dtype=F32), back, home)
    return (last.astype(BF), next_state)


def solution(mesh):
    devices = mesh.devices.reshape(NZ, NX, NY, NC)
    kv, tp = ("z", "x"), TP
    in_specs = (
        P(tp, kv),
        P(kv),
        P(kv, tp),
        P(kv, tp),
        P(kv, tp),
        P(kv, tp),
        P(tp),
        P(tp, None),
        P(kv, tp, None, None),
        P(tp, kv),
        P(kv),
        P(kv, tp),
        P(tp, kv),
    )
    out_specs = (P(tp, kv), P(kv, tp, None, None))
    return jax.shard_map(
        body, mesh=Mesh(devices, AXES), in_specs=in_specs, out_specs=out_specs, check_vma=False
    )
```

time: 129 us -> 180 us (1.40)
  waiting for transfers between devices: 37 us -> 75 us
  starting transfers between devices: 61.3 us -> 70.7 us
  other arithmetic: 11 us -> 3.48 us
  local copies, waits for them, and re-layouts: 5.97 us -> 12.8 us
  Pallas kernels: 10.1 us -> 15.7 us
    all_to_all x0 -> x9, waiting for transfers between devices: none -> 65.1 us  [exchange(): return lax.all_to_all(tiles, axis, 0, 0, tiled=True)]
    all_to_all x0 -> x9, starting transfers between devices: none -> 49.5 us  [exchange(): return lax.all_to_all(tiles, axis, 0, 0, tiled=True)]
    ppermute x39 -> x8, starting transfers between devices: 61.3 us -> 21.2 us  [send(): return lax.ppermute(value, AXES, pairs)]
    ppermute x39 -> x8, waiting for transfers between devices: 37 us -> 9.84 us  [send(): return lax.ppermute(value, AXES, pairs)]
    pallas_call x4 -> x7, Pallas kernels: 10.1 us -> 15.7 us  [call(): pl.pallas_call(kernel, out_shape=outs, in_specs=in_specs, out_specs=jax.t...]
    add x4 -> x0, other arithmetic: 3.97 us -> none  [the longest x1 2.11 us: body(): forget[..., None] * recur_state]
    broadcast_in_dim x0 -> x6, local copies, waits for them, and re-layouts: none -> 3.71 us  [the longest x4 3.68 us: gathered(): return exchange(jnp.broadcast_to(value[None], (size, *value.shape)), axis)]
    unnamed x73 -> x42, local copies, waits for them, and re-layouts: 5.08 us -> 7.47 us
  transfers between devices with their start and end apart: 39 -> 17, of which waited for: 15 -> 13; matrix products, arithmetic and copies ran while one was open for 7% -> 3% of each run, Pallas kernels for 6% -> 4%
where the time goes in v2:
time: 180 us; the launch traced here: 179 us
  waiting for transfers between devices  75 us (42%)
  starting transfers between devices  70.7 us (39%)
  Pallas kernels  15.7 us (9%)
  local copies, waits for them, and re-layouts  12.8 us (7%)
  other arithmetic  3.48 us (2%)
    all_to_all x9, waiting for transfers between devices, exchange(): return lax.all_to_all(tiles, axis, 0, 0, tiled=True)  65.1 us
    all_to_all x9, starting transfers between devices, exchange(): return lax.all_to_all(tiles, axis, 0, 0, tiled=True)  49.5 us
    ppermute x8, starting transfers between devices, send(): return lax.ppermute(value, AXES, pairs)  21.2 us
    pallas_call x7, Pallas kernels, call(): pl.pallas_call(kernel, out_shape=outs, in_specs=in_specs, out_specs=jax.t...  15.7 us
    ppermute x8, waiting for transfers between devices, send(): return lax.ppermute(value, AXES, pairs)  9.84 us
    unnamed x42, local copies, waits for them, and re-layouts  7.47 us
    broadcast_in_dim x4, local copies, waits for them, and re-layouts, gathered(): return exchange(jnp.broadcast_to(value[None], (size, *value.shape)), axis)  3.68 us
  transfers between devices with their start and end apart: 17, of which 13 were waited for; matrix products, arithmetic and copies ran while one was open for 3% of the time, Pallas kernels for 4%

profile of v2, /device:TPU:16, one launch (start us, length us, event | category | flops | bytes accessed | tf_op | source)
XLA Modules:
  0.0 178.6 jit_solution(5590519292593266746)
XLA Ops:
  0.6 0.7 reshape.80
  1.4 0.8 reshape.86
  2.2 7.4 %all-to-all-start = ((bf16[32,2,512]{2,1,0:T(2,128)(2,1)}), bf16[32,2,512]{2,1,0:T(2,128)(2,1)S(1)}, u32[]{:S(2)}, u32[]{:S(2)}) async-start(bf16[32,2,512]{2,1,0:T(2,128)(2,1)} %reshape.86), calls=%async_computation | async-start | bytes 131072 | tf_op jit(solution)/shard_map/all_to_all | solution.py:40
  9.6 0.9 multiply_convert_fusion.1
  10.5 4.4 %all-to-all-done = bf16[32,2,512]{2,1,0:T(2,128)(2,1)S(1)} async-done(((bf16[32,2,512]{2,1,0:T(2,128)(2,1)}), bf16[32,2,512]{2,1,0:T(2,128)(2,1)S(1)}, u32[]{:S(2)}, u32[]{:S(2)}) %all-to-all-start) | async-done | bytes 65568 | tf_op jit(solution)/shard_map/all_to_all | solution.py:40
  14.9 0.9 broadcast_in_dim.17
  15.7 3.5 %all-to-all-start.1 = ((bf16[4,64,1024]{2,1,0:T(8,128)(2,1)}), bf16[4,64,1024]{2,1,0:T(8,128)(2,1)S(1)}, u32[]{:S(2)}, u32[]{:S(2)}) async-start(bf16[4,64,1024]{2,1,0:T(8,128)(2,1)} %broadcast_in_dim.17), calls=%async_computation.1 | async-start | bytes 1048576 | tf_op jit(solution)/shard_map/all_to_all | solution.py:40
  19.2 0.8 reshape.87
  20.0 9.2 %all-to-all-done.1.w = bf16[4,64,1024]{2,1,0:T(8,128)(2,1)S(1)} async-done(((bf16[4,64,1024]{2,1,0:T(8,128)(2,1)}), bf16[4,64,1024]{2,1,0:T(8,128)(2,1)S(1)}, u32[]{:S(2)}, u32[]{:S(2)}) %all-to-all-start.1) | async-done | bytes 524320 | tf_op jit(solution)/shard_map/all_to_all | solution.py:40
  29.2 0.8 copy-done.2
  30.0 2.2 %shard_map.140 = bf16[8,16,1024]{2,1,0:T(8,128)(2,1)} custom-call(bf16[4,8,16,64]{3,2,1,0:T(8,128)(2,1)} %bitcast.11, bf16[4,64,1024]{2,1,0:T(8,128)(2,1)} %copy-done.2), custom_call_target="tpu_custom_call" | custom-call | tf_op jit(solution)/shard_map/pallas_call | solution.py:84
  32.2 8.5 %all-to-all-start.2 = ((bf16[8,16,1024]{2,1,0:T(8,128)(2,1)}), bf16[8,16,1024]{2,1,0:T(8,128)(2,1)S(1)}, u32[]{:S(2)}, u32[]{:S(2)}) async-start(bf16[8,16,1024]{2,1,0:T(8,128)(2,1)} %shard_map.140), calls=%async_computation.2 | async-start | bytes 524288 | tf_op jit(solution)/shard_map/all_to_all | solution.py:40
  40.7 9.7 %collective-permute-start.3 = (bf16[48,64]{1,0:T(8,128)(2,1)S(1)}, bf16[48,64]{1,0:T(8,128)(2,1)S(1)}, u32[]{:S(2)}, u32[]{:S(2)}) collective-permute-start(bf16[48,64]{1,0:T(8,128)(2,1)S(1)} %copy-done.13), channel_id=1, source_target_pairs={{0,0},{1,32},{2,64},{3,96},{4,128},{5,160},{6,192},{7,224},{8,8},{... | collective-permute-start | bytes 18440 | tf_op jit(solution)/shard_map/ppermute | solution.py:28
  50.4 1.8 %all-to-all-done.2.msg = bf16[8,16,1024]{2,1,0:T(8,128)(2,1)S(1)} async-done(((bf16[8,16,1024]{2,1,0:T(8,128)(2,1)}), bf16[8,16,1024]{2,1,0:T(8,128)(2,1)S(1)}, u32[]{:S(2)}, u32[]{:S(2)}) %all-to-all-start.2) | async-done | bytes 262176 | tf_op jit(solution)/shard_map/all_to_all | solution.py:40
  52.3 0.8 broadcast_in_dim.18
  53.0 3.4 %all-to-all-start.3 = ((bf16[8,64,256]{2,1,0:T(8,128)(2,1)}), bf16[8,64,256]{2,1,0:T(8,128)(2,1)S(1)}, u32[]{:S(2)}, u32[]{:S(2)}) async-start(bf16[8,64,256]{2,1,0:T(8,128)(2,1)} %broadcast_in_dim.18), calls=%async_computation.3 | async-start | bytes 524288 | tf_op jit(solution)/shard_map/all_to_all | solution.py:40
  57.2 3.8 %shard_map.141 = (bf16[16,256]{1,0:T(8,128)(2,1)}, f32[12,2,128,128]{3,2,1,0:T(8,128)}) custom-call(s32[1]{0:T(128)} %bitcast.1.place, bf16[8,16,1024]{2,1,0:T(8,128)(2,1)} %copy-done.4, f32[12,2,128,128]{3,2,1,0:T(8,128)} %state.1, f32[1,256]{1,0:T(1,128)} %bitcast.17, f32[2,128]{1,0:T(2,128)} %gain.1), custom_call_target="tpu_custom_call" | custom-call | tf_op jit(solution)/shard_map/pallas_call | solution.py:84
  61.5 2.1 %collective-permute-start.1 = (bf16[16,256]{1,0:T(8,128)(2,1)}, bf16[16,256]{1,0:T(8,128)(2,1)S(1)}, u32[]{:S(2)}, u32[]{:S(2)}) collective-permute-start(bf16[16,256]{1,0:T(8,128)(2,1)} %get-tuple-element.11.m0), channel_id=1, source_target_pairs={{0,16},{1,17},{2,18},{3,19},{4,20},{5,21},{6,22},{7,23},{8,24},{9,... | collective-permute-start | bytes 24584 | tf_op jit(solution)/shard_map/ppermute | solution.py:28
  64.2 0.6 fusion.tok
  64.8 2.0 %all-to-all-done.3.w = bf16[8,64,256]{2,1,0:T(8,128)(2,1)S(1)} async-done(((bf16[8,64,256]{2,1,0:T(8,128)(2,1)}), bf16[8,64,256]{2,1,0:T(8,128)(2,1)S(1)}, u32[]{:S(2)}, u32[]{:S(2)}) %all-to-all-start.3) | async-done | bytes 262176 | tf_op jit(solution)/shard_map/all_to_all | solution.py:40
  68.2 2.0 %shard_map.142 = bf16[8,48,512]{2,1,0:T(8,128)(2,1)} custom-call(s32[4]{0:T(128)} %and_select_fusion.row_at, bf16[16,256]{1,0:T(8,128)(2,1)} %get-tuple-element.11.m0, bf16[16,256]{1,0:T(8,128)(2,1)} %copy-done.17, bf16[16,256]{1,0:T(8,128)(2,1)} %copy-done.16, bf16[16,256]{1,0:T(8,128)(2,1)} %copy-done.15, bf16[8,64,256]{2,1,0:T(8,128)(2,1)} %copy-done.6, ...), custom_call_target="tpu_custom_call" | custom-call | tf_op jit(solution)/shard_map/pallas_call | solution.py:84
  70.2 5.6 %all-to-all-start.4 = ((bf16[8,48,512]{2,1,0:T(8,128)(2,1)}), bf16[8,48,512]{2,1,0:T(8,128)(2,1)S(1)}, u32[]{:S(2)}, u32[]{:S(2)}) async-start(bf16[8,48,512]{2,1,0:T(8,128)(2,1)} %shard_map.142), calls=%async_computation.4 | async-start | bytes 786432 | tf_op jit(solution)/shard_map/all_to_all | solution.py:40
  75.8 5.6 %all-to-all-done.4.parts = bf16[8,48,512]{2,1,0:T(8,128)(2,1)S(1)} async-done(((bf16[8,48,512]{2,1,0:T(8,128)(2,1)}), bf16[8,48,512]{2,1,0:T(8,128)(2,1)S(1)}, u32[]{:S(2)}, u32[]{:S(2)}) %all-to-all-start.4) | async-done | bytes 393248 | tf_op jit(solution)/shard_map/all_to_all | solution.py:40
  81.5 1.1 broadcast_in_dim.20
  82.6 7.1 %all-to-all-start.5 = ((bf16[8,64,1024]{2,1,0:T(8,128)(2,1)}), bf16[8,64,1024]{2,1,0:T(8,128)(2,1)S(1)}, u32[]{:S(2)}, u32[]{:S(2)}) async-start(bf16[8,64,1024]{2,1,0:T(8,128)(2,1)} %broadcast_in_dim.20), calls=%async_computation.5 | async-start | bytes 2097152 | tf_op jit(solution)/shard_map/all_to_all | solution.py:40
  89.7 28.8 %all-to-all-done.5.w = bf16[8,64,1024]{2,1,0:T(8,128)(2,1)S(1)} async-done(((bf16[8,64,1024]{2,1,0:T(8,128)(2,1)}), bf16[8,64,1024]{2,1,0:T(8,128)(2,1)S(1)}, u32[]{:S(2)}, u32[]{:S(2)}) %all-to-all-start.5) | async-done | bytes 1048608 | tf_op jit(solution)/shard_map/all_to_all | solution.py:40
  118.4 0.9 broadcast_in_dim.21
  119.4 3.9 %all-to-all-start.7 = ((bf16[4,64,1024]{2,1,0:T(8,128)(2,1)}), bf16[4,64,1024]{2,1,0:T(8,128)(2,1)S(1)}, u32[]{:S(2)}, u32[]{:S(2)}) async-start(bf16[4,64,1024]{2,1,0:T(8,128)(2,1)} %broadcast_in_dim.21), calls=%async_computation.7 | async-start | bytes 1048576 | tf_op jit(solution)/shard_map/all_to_all | solution.py:40
  123.3 2.4 %shard_map.143 = (bf16[48,512]{1,0:T(8,128)(2,1)}, bf16[16,1024]{1,0:T(8,128)(2,1)}, bf16[16,1024]{1,0:T(8,128)(2,1)}, bf16[16,1024]{1,0:T(8,128)(2,1)}, bf16[16,1024]{1,0:T(8,128)(2,1)}) custom-call(s32[4]{0:T(128)} %and_select_fusion.row_at, bf16[8,48,512]{2,1,0:T(8,128)(2,1)} %copy-done.3, bf16[8,64,1024]{2,1,0:T(8,128)(2,1)} %copy-done), custom_call_target="tpu_custom_call" | custom-call | tf_op jit(solution)/shard_map/pallas_call | solution.py:84
  125.8 2.0 %collective-permute-start.4 = (bf16[16,1024]{1,0:T(8,128)(2,1)}, bf16[16,1024]{1,0:T(8,128)(2,1)S(1)}, u32[]{:S(2)}, u32[]{:S(2)}) collective-permute-start(bf16[16,1024]{1,0:T(8,128)(2,1)} %get-tuple-element.14), channel_id=1, source_target_pairs={{0,8},{1,9},{2,10},{3,11},{4,12},{5,13},{6,14},{7,15},{8,16},{9,17... | collective-permute-start | bytes 98312 | tf_op jit(solution)/shard_map/ppermute | solution.py:28
  127.8 2.7 %collective-permute-start.5 = (bf16[16,1024]{1,0:T(8,128)(2,1)}, bf16[16,1024]{1,0:T(8,128)(2,1)S(1)}, u32[]{:S(2)}, u32[]{:S(2)}) collective-permute-start(bf16[16,1024]{1,0:T(8,128)(2,1)} %get-tuple-element.15), channel_id=1, source_target_pairs={{0,16},{1,17},{2,18},{3,19},{4,20},{5,21},{6,22},{7,23},{8,24},{9,... | collective-permute-start | bytes 98312 | tf_op jit(solution)/shard_map/ppermute | solution.py:28
  130.5 1.5 collective-permute-start.6
  131.9 1.8 %collective-permute-done.4.m1 = bf16[16,1024]{1,0:T(8,128)(2,1)S(1)} collective-permute-done((bf16[16,1024]{1,0:T(8,128)(2,1)}, bf16[16,1024]{1,0:T(8,128)(2,1)S(1)}, u32[]{:S(2)}, u32[]{:S(2)}) %collective-permute-start.4) | collective-permute-done | bytes 32800 | tf_op jit(solution)/shard_map/ppermute | solution.py:28
  133.7 0.6 collective-permute-done.5.m2
  135.2 1.6 shard_map.144
  136.8 3.4 %all-to-all-start.6 = ((bf16[8,16,1024]{2,1,0:T(8,128)(2,1)}), bf16[8,16,1024]{2,1,0:T(8,128)(2,1)S(1)}, u32[]{:S(2)}, u32[]{:S(2)}) async-start(bf16[8,16,1024]{2,1,0:T(8,128)(2,1)} %shard_map.144), calls=%async_computation.6 | async-start | bytes 524288 | tf_op jit(solution)/shard_map/all_to_all | solution.py:40
  140.2 10.9 %all-to-all-done.6.hidden = bf16[8,16,1024]{2,1,0:T(8,128)(2,1)S(1)} async-done(((bf16[8,16,1024]{2,1,0:T(8,128)(2,1)}), bf16[8,16,1024]{2,1,0:T(8,128)(2,1)S(1)}, u32[]{:S(2)}, u32[]{:S(2)}) %all-to-all-start.6) | async-done | bytes 262176 | tf_op jit(solution)/shard_map/all_to_all | solution.py:40
  151.2 0.7 copy-done.5
  151.9 2.1 %shard_map.145 = bf16[4,8,16,64]{3,2,1,0:T(8,128)(2,1)} custom-call(bf16[8,16,1024]{2,1,0:T(8,128)(2,1)} %copy-done.5, bf16[4,64,1024]{2,1,0:T(8,128)(2,1)} %copy-done.1), custom_call_target="tpu_custom_call" | custom-call | tf_op jit(solution)/shard_map/pallas_call | solution.py:84
  154.0 1.7 reshape.88
  155.7 6.8 %all-to-all-start.8 = ((bf16[32,2,512]{2,1,0:T(2,128)(2,1)}), bf16[32,2,512]{2,1,0:T(2,128)(2,1)S(1)}, u32[]{:S(2)}, u32[]{:S(2)}) async-start(bf16[32,2,512]{2,1,0:T(2,128)(2,1)} %reshape.88), calls=%async_computation.8 | async-start | bytes 131072 | tf_op jit(solution)/shard_map/all_to_all | solution.py:40
  162.4 0.8 constant_dynamic-slice_fusion
  163.2 2.1 %collective-permute-start.7 = (bf16[48,64]{1,0:T(8,128)(2,1)S(1)}, bf16[48,64]{1,0:T(8,128)(2,1)S(1)}, u32[]{:S(2)}, u32[]{:S(2)}) collective-permute-start(bf16[48,64]{1,0:T(8,128)(2,1)S(1)} %constant_dynamic-slice_fusion), channel_id=1, source_target_pairs={{0,0},{1,32},{2,64},{3,96},{4,128},{5,160},{6,192},{7,224},{8,8},{... | collective-permute-start | bytes 18440 | tf_op jit(solution)/shard_map/ppermute | solution.py:28
  165.4 2.4 %all-to-all-done.8 = bf16[32,2,512]{2,1,0:T(2,128)(2,1)S(1)} async-done(((bf16[32,2,512]{2,1,0:T(2,128)(2,1)}), bf16[32,2,512]{2,1,0:T(2,128)(2,1)S(1)}, u32[]{:S(2)}, u32[]{:S(2)}) %all-to-all-start.8) | async-done | bytes 65568 | tf_op jit(solution)/shard_map/all_to_all | solution.py:40
  167.8 0.8 reshape.89
  168.5 6.6 %collective-permute-done.7.mixed = bf16[48,64]{1,0:T(8,128)(2,1)S(1)} collective-permute-done((bf16[48,64]{1,0:T(8,128)(2,1)S(1)}, bf16[48,64]{1,0:T(8,128)(2,1)S(1)}, u32[]{:S(2)}, u32[]{:S(2)}) %collective-permute-start.7) | collective-permute-done | bytes 6176 | tf_op jit(solution)/shard_map/ppermute | solution.py:28
  175.7 1.5 shard_map.146
  177.3 1.3 convert_element_type.29
  (52 shorter events, 4.8 us)
Async XLA Ops:
  2.2 12.7 %all-to-all-start = ((bf16[32,2,512]{2,1,0:T(2,128)(2,1)}), bf16[32,2,512]{2,1,0:T(2,128)(2,1)S(1)}, u32[]{:S(2)}, u32[]{:S(2)}) async-start(bf16[32,2,512]{2,1,0:T(2,128)(2,1)} %reshape.86), calls=%async_computation | async-start | bytes 131072 | tf_op jit(solution)/shard_map/all_to_all | solution.py:40
  10.5 30.2 %copy-start.13 = (bf16[48,64]{1,0:T(8,128)(2,1)S(1)}, bf16[48,64]{1,0:T(8,128)(2,1)}, u32[]{:S(2)}) copy-start(bf16[48,64]{1,0:T(8,128)(2,1)} %param.13) | copy-start | bytes 18436
  10.5 41.8 %copy-start.9 = (bf16[256,64]{0,1:T(8,128)(2,1)S(1)}, bf16[256,64]{0,1:T(8,128)(2,1)}, u32[]{:S(2)}) copy-start(bf16[256,64]{0,1:T(8,128)(2,1)} %param.22) | copy-start | bytes 98308
  15.7 13.5 %all-to-all-start.1 = ((bf16[4,64,1024]{2,1,0:T(8,128)(2,1)}), bf16[4,64,1024]{2,1,0:T(8,128)(2,1)S(1)}, u32[]{:S(2)}, u32[]{:S(2)}) async-start(bf16[4,64,1024]{2,1,0:T(8,128)(2,1)} %broadcast_in_dim.17), calls=%async_computation.1 | async-start | bytes 1048576 | tf_op jit(solution)/shard_map/all_to_all | solution.py:40
  29.2 0.8 copy-start.2
  32.2 20.0 %all-to-all-start.2 = ((bf16[8,16,1024]{2,1,0:T(8,128)(2,1)}), bf16[8,16,1024]{2,1,0:T(8,128)(2,1)S(1)}, u32[]{:S(2)}, u32[]{:S(2)}) async-start(bf16[8,16,1024]{2,1,0:T(8,128)(2,1)} %shard_map.140), calls=%async_computation.2 | async-start | bytes 524288 | tf_op jit(solution)/shard_map/all_to_all | solution.py:40
  40.7 16.3 %collective-permute-start.3 = (bf16[48,64]{1,0:T(8,128)(2,1)S(1)}, bf16[48,64]{1,0:T(8,128)(2,1)S(1)}, u32[]{:S(2)}, u32[]{:S(2)}) collective-permute-start(bf16[48,64]{1,0:T(8,128)(2,1)S(1)} %copy-done.13), channel_id=1, source_target_pairs={{0,0},{1,32},{2,64},{3,96},{4,128},{5,160},{6,192},{7,224},{8,8},{... | collective-permute-start | bytes 18440 | tf_op jit(solution)/shard_map/ppermute | solution.py:28
  52.3 4.9 %copy-start.4 = (bf16[8,16,1024]{2,1,0:T(8,128)(2,1)}, bf16[8,16,1024]{2,1,0:T(8,128)(2,1)S(1)}, u32[]{:S(2)}) copy-start(bf16[8,16,1024]{2,1,0:T(8,128)(2,1)S(1)} %all-to-all-done.2.msg) | copy-start | bytes 786436
  53.0 13.8 %all-to-all-start.3 = ((bf16[8,64,256]{2,1,0:T(8,128)(2,1)}), bf16[8,64,256]{2,1,0:T(8,128)(2,1)S(1)}, u32[]{:S(2)}, u32[]{:S(2)}) async-start(bf16[8,64,256]{2,1,0:T(8,128)(2,1)} %broadcast_in_dim.18), calls=%async_computation.3 | async-start | bytes 524288 | tf_op jit(solution)/shard_map/all_to_all | solution.py:40
  57.2 18.6 %copy-start.8 = (bf16[64,1024]{1,0:T(8,128)(2,1)S(1)}, bf16[64,1024]{1,0:T(8,128)(2,1)}, u32[]{:S(2)}) copy-start(bf16[64,1024]{1,0:T(8,128)(2,1)} %param.24) | copy-start | bytes 393220
  57.2 18.6 %copy-start.18 = (f32[64]{0:T(128)S(1)}, f32[64]{0:T(128)}, u32[]{:S(2)}) copy-start(f32[64]{0:T(128)} %param.23) | copy-start | bytes 772
  61.0 5.9 %collective-permute-start.2 = (bf16[16,256]{1,0:T(8,128)(2,1)}, bf16[16,256]{1,0:T(8,128)(2,1)S(1)}, u32[]{:S(2)}, u32[]{:S(2)}) collective-permute-start(bf16[16,256]{1,0:T(8,128)(2,1)} %get-tuple-element.11.m0), channel_id=1, source_target_pairs={{0,8},{1,9},{2,10},{3,11},{4,12},{5,13},{6,14},{7,15},{8,16},{9,17... | collective-permute-start | bytes 24584 | tf_op jit(solution)/shard_map/ppermute | solution.py:28
  61.5 5.4 %collective-permute-start.1 = (bf16[16,256]{1,0:T(8,128)(2,1)}, bf16[16,256]{1,0:T(8,128)(2,1)S(1)}, u32[]{:S(2)}, u32[]{:S(2)}) collective-permute-start(bf16[16,256]{1,0:T(8,128)(2,1)} %get-tuple-element.11.m0), channel_id=1, source_target_pairs={{0,16},{1,17},{2,18},{3,19},{4,20},{5,21},{6,22},{7,23},{8,24},{9,... | collective-permute-start | bytes 24584 | tf_op jit(solution)/shard_map/ppermute | solution.py:28
  63.6 3.9 %collective-permute-start = (bf16[16,256]{1,0:T(8,128)(2,1)}, bf16[16,256]{1,0:T(8,128)(2,1)S(1)}, u32[]{:S(2)}, u32[]{:S(2)}) collective-permute-start(bf16[16,256]{1,0:T(8,128)(2,1)} %get-tuple-element.11.m0), channel_id=1, source_target_pairs={{0,24},{1,25},{2,26},{3,27},{4,28},{5,29},{6,30},{7,31},{8,0},{9,1... | collective-permute-start | bytes 24584 | tf_op jit(solution)/shard_map/ppermute | solution.py:28
  66.8 0.7 copy-start.6
  66.9 0.7 copy-start.15
  66.9 0.7 copy-start.16
  67.6 0.6 copy-start.17
  70.2 11.3 %all-to-all-start.4 = ((bf16[8,48,512]{2,1,0:T(8,128)(2,1)}), bf16[8,48,512]{2,1,0:T(8,128)(2,1)S(1)}, u32[]{:S(2)}, u32[]{:S(2)}) async-start(bf16[8,48,512]{2,1,0:T(8,128)(2,1)} %shard_map.142), calls=%async_computation.4 | async-start | bytes 786432 | tf_op jit(solution)/shard_map/all_to_all | solution.py:40
  75.8 42.6 %copy-start.7 = (bf16[1024,64]{0,1:T(8,128)(2,1)S(1)}, bf16[1024,64]{0,1:T(8,128)(2,1)}, u32[]{:S(2)}) copy-start(bf16[1024,64]{0,1:T(8,128)(2,1)} %param.25) | copy-start | bytes 393220
  81.5 1.1 copy-start.3
  82.6 35.8 %all-to-all-start.5 = ((bf16[8,64,1024]{2,1,0:T(8,128)(2,1)}), bf16[8,64,1024]{2,1,0:T(8,128)(2,1)S(1)}, u32[]{:S(2)}, u32[]{:S(2)}) async-start(bf16[8,64,1024]{2,1,0:T(8,128)(2,1)} %broadcast_in_dim.20), calls=%async_computation.5 | async-start | bytes 2097152 | tf_op jit(solution)/shard_map/all_to_all | solution.py:40
  118.4 4.9 %copy-start = (bf16[8,64,1024]{2,1,0:T(8,128)(2,1)}, bf16[8,64,1024]{2,1,0:T(8,128)(2,1)S(1)}, u32[]{:S(2)}) copy-start(bf16[8,64,1024]{2,1,0:T(8,128)(2,1)S(1)} %all-to-all-done.5.w) | copy-start | bytes 3145732
  119.4 17.5 %all-to-all-start.7 = ((bf16[4,64,1024]{2,1,0:T(8,128)(2,1)}), bf16[4,64,1024]{2,1,0:T(8,128)(2,1)S(1)}, u32[]{:S(2)}, u32[]{:S(2)}) async-start(bf16[4,64,1024]{2,1,0:T(8,128)(2,1)} %broadcast_in_dim.21), calls=%async_computation.7 | async-start | bytes 1048576 | tf_op jit(solution)/shard_map/all_to_all | solution.py:40
  125.8 8.0 %collective-permute-start.4 = (bf16[16,1024]{1,0:T(8,128)(2,1)}, bf16[16,1024]{1,0:T(8,128)(2,1)S(1)}, u32[]{:S(2)}, u32[]{:S(2)}) collective-permute-start(bf16[16,1024]{1,0:T(8,128)(2,1)} %get-tuple-element.14), channel_id=1, source_target_pairs={{0,8},{1,9},{2,10},{3,11},{4,12},{5,13},{6,14},{7,15},{8,16},{9,17... | collective-permute-start | bytes 98312 | tf_op jit(solution)/shard_map/ppermute | solution.py:28
  127.8 6.6 %collective-permute-start.5 = (bf16[16,1024]{1,0:T(8,128)(2,1)}, bf16[16,1024]{1,0:T(8,128)(2,1)S(1)}, u32[]{:S(2)}, u32[]{:S(2)}) collective-permute-start(bf16[16,1024]{1,0:T(8,128)(2,1)} %get-tuple-element.15), channel_id=1, source_target_pairs={{0,16},{1,17},{2,18},{3,19},{4,20},{5,21},{6,22},{7,23},{8,24},{9,... | collective-permute-start | bytes 98312 | tf_op jit(solution)/shard_map/ppermute | solution.py:28
  130.5 4.1 %collective-permute-start.6 = (bf16[16,1024]{1,0:T(8,128)(2,1)}, bf16[16,1024]{1,0:T(8,128)(2,1)S(1)}, u32[]{:S(2)}, u32[]{:S(2)}) collective-permute-start(bf16[16,1024]{1,0:T(8,128)(2,1)} %get-tuple-element.16), channel_id=1, source_target_pairs={{0,24},{1,25},{2,26},{3,27},{4,28},{5,29},{6,30},{7,31},{8,0},{9,1... | collective-permute-start | bytes 98312 | tf_op jit(solution)/shard_map/ppermute | solution.py:28
  133.7 0.9 copy-start.10
  134.4 0.6 copy-start.11
  134.6 0.6 copy-start.12
  136.8 14.3 %copy-start.1 = (bf16[4,64,1024]{2,1,0:T(8,128)(2,1)}, bf16[4,64,1024]{2,1,0:T(8,128)(2,1)S(1)}, u32[]{:S(2)}) copy-start(bf16[4,64,1024]{2,1,0:T(8,128)(2,1)S(1)} %all-to-all-done.7.w) | copy-start | bytes 1572868
  136.8 14.3 %all-to-all-start.6 = ((bf16[8,16,1024]{2,1,0:T(8,128)(2,1)}), bf16[8,16,1024]{2,1,0:T(8,128)(2,1)S(1)}, u32[]{:S(2)}, u32[]{:S(2)}) async-start(bf16[8,16,1024]{2,1,0:T(8,128)(2,1)} %shard_map.144), calls=%async_computation.6 | async-start | bytes 524288 | tf_op jit(solution)/shard_map/all_to_all | solution.py:40
  151.2 0.7 copy-start.5
  155.7 12.1 %all-to-all-start.8 = ((bf16[32,2,512]{2,1,0:T(2,128)(2,1)}), bf16[32,2,512]{2,1,0:T(2,128)(2,1)S(1)}, u32[]{:S(2)}, u32[]{:S(2)}) async-start(bf16[32,2,512]{2,1,0:T(2,128)(2,1)} %reshape.88), calls=%async_computation.8 | async-start | bytes 131072 | tf_op jit(solution)/shard_map/all_to_all | solution.py:40
  163.2 11.9 %collective-permute-start.7 = (bf16[48,64]{1,0:T(8,128)(2,1)S(1)}, bf16[48,64]{1,0:T(8,128)(2,1)S(1)}, u32[]{:S(2)}, u32[]{:S(2)}) collective-permute-start(bf16[48,64]{1,0:T(8,128)(2,1)S(1)} %constant_dynamic-slice_fusion), channel_id=1, source_target_pairs={{0,0},{1,32},{2,64},{3,96},{4,128},{5,160},{6,192},{7,224},{8,8},{... | collective-permute-start | bytes 18440 | tf_op jit(solution)/shard_map/ppermute | solution.py:28
  175.1 0.6 copy-start.14

commit v3 on v2

v3 whole, which is shorter than its diff:
```python
import jax
import jax.numpy as jnp
from jax import lax
from jax.experimental import pallas as pl
from jax.experimental.pallas import tpu as pltpu
from jax.sharding import Mesh, PartitionSpec as P


NORM_EPS = 1e-05
NZ, NX, NY, NC = 8, 4, 4, 2
NT = NY * NC
AXES = ("z", "x", "y", "core")
TP = ("y", "core")
XTP = ("x", "y", "core")
BF, F32 = jnp.bfloat16, jnp.float32


def flat(z, x, y, c):
    return ((z * NX + x) * NY + y) * NC + c


def send(value, to):
    pairs = []
    for z in range(NZ):
        for x in range(NX):
            for y in range(NY):
                for c in range(NC):
                    pairs.append((flat(z, x, y, c), flat(*to(z, x, y, c))))
    return lax.ppermute(value, AXES, pairs)


def to_z(value, k):
    return send(value, lambda z, x, y, c: ((z + k) % NZ, x, y, c))


def to_x(value, k):
    return send(value, lambda z, x, y, c: (z, (x + k) % NX, y, c))


def to_y(value, k):
    return send(value, lambda z, x, y, c: (z, x, (y + k) % NY, c))


def to_core(value):
    return send(value, lambda z, x, y, c: (z, x, y, 1 - c))


def swap_rows(value):
    return send(value, lambda z, x, y, c: (NC * y + c, x, z // NC, z % NC))


def exchange(tiles, axis):
    return lax.all_to_all(tiles, axis, 0, 0, tiled=True)


def after(value, *others):
    return lax.optimization_barrier((value, *others))[0]


def nt(a, b, precision=None):
    return lax.dot_general(
        a, b, (((1,), (1,)), ((), ())), preferred_element_type=F32, precision=precision
    )


def nn(a, b):
    return jnp.dot(a, b, preferred_element_type=F32)


def with_squares(main, rows):
    n = main.shape[0] // 16
    sums = nt(jnp.ones((8, rows.shape[1]), F32), rows * rows, lax.Precision.HIGHEST)[:1]
    high = sums.astype(BF).astype(F32)
    low = sums - high
    row = lax.broadcasted_iota(jnp.int32, (n, 16, 128), 1)
    cube = main.reshape(n, 16, 1024)
    head = jnp.where(row == 12, high[None], jnp.where(row == 13, low[None], cube[:, :, :128]))
    return jnp.concatenate([head, cube[:, :, 128:]], axis=2).astype(BF)


def scaled(total, place):
    sums = total[12:13, :128] + total[13:14, :128]
    row = lax.broadcasted_iota(jnp.int32, (16, 128), 0)
    lane = lax.broadcasted_iota(jnp.int32, (16, 128), 1)
    mine = jnp.where((lane == row + 16 * place) & (row < 12), sums, 0.0)
    square = jnp.sum(mine, axis=1, keepdims=True)
    return total * lax.rsqrt(square / 2048 + NORM_EPS)


def lane_squares(v):
    s = v * v
    return (s[:, 0:128] + s[:, 128:256]) + (s[:, 256:384] + s[:, 384:512])


def call(kernel, outs, *args, scratch=()):
    in_specs = [
        pl.BlockSpec(memory_space=pltpu.SMEM if a.dtype == jnp.int32 else pltpu.VMEM) for a in args
    ]
    args = [
        a if a.dtype == jnp.int32 else pltpu.with_memory_space_constraint(a, pltpu.VMEM)
        for a in args
    ]
    return pl.pallas_call(
        kernel,
        out_shape=outs,
        in_specs=in_specs,
        out_specs=jax.tree.map(lambda _: pl.BlockSpec(memory_space=pltpu.VMEM), outs),
        scratch_shapes=scratch,
    )(*args)


def shape(*dims, dtype=BF):
    return jax.ShapeDtypeStruct(dims, dtype)


def local(*dims, dtype=BF):
    return pltpu.VMEM(dims, dtype)


def spread_kernel(tok, out):
    wide = tok[...].astype(F32)
    pad = jnp.zeros((4, 64), F32)
    for i in range(NX):
        rows = jnp.concatenate([wide[12 * i : 12 * i + 12], pad], axis=0)
        tile = jnp.concatenate([rows[:8], rows[8:]], axis=1).astype(BF)
        for k in range(NT):
            out[NT * i + k] = tile


def fold_kernel(wq, wf, wi, wg, gain, out):
    for k, w in enumerate((wq, wf, wi, wg)):
        out[:, 256 * k : 256 * k + 256] = (w[...].astype(F32) * gain[...]).astype(BF)


def project_kernel(x_at, tok, w0, w1, w2, w3, out, both):
    for i in range(NX):
        part = tok[NT * i : NT * i + NT]
        both[i] = jnp.concatenate([part[:, :, :64], part[:, :, 64:]], axis=1).reshape(128, 64)
    x = jnp.concatenate([both[x_at[k]] for k in range(NX)], axis=1)
    main = nn(x, jnp.concatenate([w[...] for w in (w0, w1, w2, w3)], axis=0))
    out[...] = with_squares(main, x.astype(F32))


def recur_kernel(place, msg, bound, gain, state_hbm, mixture, new_hbm, state, new, came, went):
    reading = [pltpu.make_async_copy(state_hbm.at[r], state.at[r], came.at[r]) for r in range(12)]
    writing = [pltpu.make_async_copy(new.at[r], new_hbm.at[r], went.at[r]) for r in range(12)]
    for copy in reading:
        copy.start()
    total = msg[0].astype(F32)
    for k in range(1, NZ):
        total = total + msg[k].astype(F32)
    total = scaled(total, place[0])
    reads = [[], []]
    low = bound[...]
    forget = low + (1.0 - low) * jax.nn.sigmoid(total[:, 256:512])
    f_t = [forget[:, :128].T, forget[:, 128:].T]
    q_t = [total[:, :128].T, total[:, 128:256].T]
    v = total[:, 512:768]
    for r in range(12):
        reading[r].wait()
        for h in range(2):
            row = v[r : r + 1, 128 * h : 128 * h + 128]
            s = row + f_t[h][:, r : r + 1] * (state[r, h] - row)
            new[r, h] = s
            reads[h].append(jnp.sum(q_t[h][:, r : r + 1] * s, axis=0, keepdims=True))
        writing[r].start()
    for h in range(2):
        at = slice(128 * h, 128 * h + 128)
        read = jnp.concatenate(reads[h] + [jnp.zeros((4, 128), F32)], axis=0)
        read = read * lax.rsqrt(jnp.mean(read * read, axis=1, keepdims=True) + NORM_EPS)
        mixture[:, at] = (read * gain[h : h + 1] * jax.nn.silu(total[:, 768:][:, at])).astype(BF)
    for copy in writing:
        copy.wait()


def attend_kernel(x_at, m0, m1, m2, m3, *rest):
    ws, (tok, out, acc) = rest[:NZ], rest[NZ:]
    for k, m in enumerate((m0, m1, m2, m3)):
        acc[x_at[k]] = m[...]
    ws = [w if w.shape[0] == 16 else w.at[128:144] for w in ws]
    w = jnp.concatenate([w[:, 256 * j : 256 * j + 256] for w in ws for j in range(4)], axis=0)
    part = nt(acc[...].reshape(64, 256), w)
    part = jnp.concatenate([part[16 * i : 16 * i + 12] for i in range(NX)], axis=0)
    out[...] = (part + tok[...].astype(F32)).astype(BF)


def pair_kernel(a, b, out):
    out[...] = (a[...].astype(F32) + b[...].astype(F32)).astype(BF)


def up_kernel(s0, s1, s2, s3, *rest):
    ws, (mixed, msg) = rest[:NZ], rest[NZ:]
    total = (s0[...].astype(F32) + s1[...].astype(F32)) + (s2[...].astype(F32) + s3[...].astype(F32))
    rows = total.astype(BF)
    mixed[...] = rows
    w = jnp.concatenate([w[:64, :] for w in ws], axis=0)
    msg[:, :1024] = nn(rows, w).astype(BF)
    msg[:, 1024:] = lane_squares(rows.astype(F32)).astype(BF)


def down_kernel(put_at, h0, h1, h2, h3, *rest):
    ws, (keep, give, acc) = rest[:NZ], rest[NZ:]
    total = (h0[...].astype(F32) + h1[...].astype(F32)) + (h2[...].astype(F32) + h3[...].astype(F32))
    scale = lax.rsqrt(jnp.sum(total[:, 1024:], axis=1, keepdims=True) / 2048 + NORM_EPS)
    hidden = jnp.square(jnp.maximum(total[:, :1024] * scale, 0.0)).astype(BF)
    part = nt(hidden, jnp.concatenate([w[...] if w.shape[0] == 64 else w[64:128, :] for w in ws], axis=0)).astype(BF)
    for k in range(NZ):
        acc[put_at[k]] = part[:, 64 * k : 64 * (k + 1)]
    keep[...] = acc[:NY]
    give[...] = acc[NY:]


def halve_kernel(kept, came, o0, o1, o2, o3):
    for k, o in enumerate((o0, o1, o2, o3)):
        o[...] = (kept[k].astype(F32) + came[k].astype(F32)).astype(BF)


def last_kernel(k_at, mixed, p0, p1, p2, p3, out, acc):
    for k in range(NZ):
        acc[k] = mixed[:, 64 * k : 64 * k + 64]
    total = (p0[...].astype(F32) + p1[...].astype(F32)) + (p2[...].astype(F32) + p3[...].astype(F32))
    out[...] = (acc[k_at[0]].astype(F32) + total).astype(BF)


def body(
    tokens, norm_gain, w_query, w_forget, w_input, w_gate, lower_bound, head_gain, recur_state,
    w_out, mixer_gain, w_up, w_down,
):
    z, x = lax.axis_index("z"), lax.axis_index("x")
    y, c = lax.axis_index("y"), lax.axis_index("core")
    t = y * NC + c
    kz = (z + jnp.arange(NZ)) % NZ
    put_at = ((kz + c) % NC * NY + (kz // NC - y) % NY).astype(jnp.int32)
    x_at = ((x + jnp.arange(NX)) % NX).astype(jnp.int32)
    z_at = z.reshape(1).astype(jnp.int32)
    k_at = ((t - z) % NZ).reshape(1).astype(jnp.int32)

    tok = exchange(call(spread_kernel, shape(NX * NT, 8, 128), tokens), XTP)
    moved = swap_rows(tokens)
    w_in = call(
        fold_kernel, local(64, 1024), w_query, w_forget, w_input, w_gate, norm_gain.reshape(64, 1)
    )
    w_ins = [w_in] + [to_x(w_in, -k) for k in range(1, NX)]

    out_t = w_out.T.reshape(4, 16, 256)
    out_t = jnp.concatenate([out_t[j] for j in range(4)], axis=1)
    w_up = (w_up.astype(F32) * mixer_gain[:, None]).astype(BF)
    bundle = jnp.concatenate([w_up, w_down.T, out_t], axis=0)
    shards = [bundle] + [None] * (NZ - 1)
    far = to_z(out_t, 4)
    up, down = bundle, bundle
    for k in (1, 2):
        up, down = to_z(up, 1), to_z(down, -1)
        shards[NZ - k], shards[k] = up, down

    parts = call(
        project_kernel, shape(NZ, 16, 1024), x_at, tok, *w_ins,
        scratch=[pltpu.VMEM((NX, 128, 64), BF)],
    )
    msg = exchange(parts, "z")
    mixture, next_state = pl.pallas_call(
        recur_kernel,
        out_shape=[local(16, 256), shape(12, 2, 128, 128, dtype=F32)],
        in_specs=[pl.BlockSpec(memory_space=pltpu.SMEM)]
        + [pl.BlockSpec(memory_space=pltpu.VMEM)] * 3
        + [pl.BlockSpec(memory_space=pl.ANY)],
        out_specs=[pl.BlockSpec(memory_space=pltpu.VMEM), pl.BlockSpec(memory_space=pl.ANY)],
        scratch_shapes=[
            pltpu.VMEM((12, 2, 128, 128), F32),
            pltpu.VMEM((12, 2, 128, 128), F32),
            pltpu.SemaphoreType.DMA((12,)),
            pltpu.SemaphoreType.DMA((12,)),
        ],
    )(
        z_at,
        pltpu.with_memory_space_constraint(msg, pltpu.VMEM),
        lower_bound.reshape(1, 256),
        head_gain,
        recur_state,
    )
    up, down = to_z(after(up, msg), 1), to_z(after(down, mixture), -1)
    shards[5], shards[3] = up, down

    mixes = [mixture] + [to_x(mixture, -k) for k in (2, 1, 3)]
    mixes = [mixes[0], mixes[2], mixes[1], mixes[3]]
    block = lax.broadcasted_iota(jnp.int32, (48, 512), 1) // 64
    spread = jnp.where(block == k_at[0], jnp.tile(moved, (1, NZ)), jnp.zeros((), BF))
    attn = call(
        attend_kernel, local(48, 512), x_at, *mixes, *shards[:4], far, *shards[5:], spread,
        scratch=[pltpu.VMEM((NX, 16, 256), BF)],
    )
    pair = to_core(attn)
    fourth_up = to_z(after(up[:64], attn), 1)
    fourth_down = to_z(after(down[64:128], attn), -1)
    duo = call(pair_kernel, local(48, 512), attn, pair)
    sums = [duo] + [to_y(duo, k) for k in (2, 1, 3)]
    mixed, wide = call(
        up_kernel, [local(48, 512), local(48, 1152)], *sums, *shards[:4], fourth_up, *shards[5:]
    )
    wides = [wide] + [to_x(wide, k) for k in (2, 1, 3)]
    keep, give = call(
        down_kernel, [local(NY, 48, 64)] * 2, put_at, *wides, *shards[:4], fourth_down, *shards[5:],
        scratch=[pltpu.VMEM((NZ, 48, 64), BF)],
    )
    lasts = call(halve_kernel, [local(48, 64)] * NY, keep, to_core(give))
    lasts = [lasts[0]] + [to_y(lasts[k], k) for k in (2, 1, 3)]
    rows = call(
        last_kernel, local(48, 64), k_at, mixed, *lasts,
        scratch=[pltpu.VMEM((NZ, 48, 64), BF)],
    )
    return (swap_rows(rows), next_state)


def solution(mesh):
    devices = mesh.devices.reshape(NZ, NX, NY, NC)
    kv, tp = ("z", "x"), TP
    in_specs = (
        P(tp, kv),
        P(kv),
        P(kv, tp),
        P(kv, tp),
        P(kv, tp),
        P(kv, tp),
        P(tp),
        P(tp, None),
        P(kv, tp, None, None),
        P(tp, kv),
        P(kv),
        P(kv, tp),
        P(tp, kv),
    )
    out_specs = (P(tp, kv), P(kv, tp, None, None))
    return jax.shard_map(
        body, mesh=Mesh(devices, AXES), in_specs=in_specs, out_specs=out_specs, check_vma=False
    )
```

time: 180 us -> 124 us (0.69)
  the two profiles are of different devices: /device:TPU:16 before, /device:TPU:88 now
where the time goes in v3:
time: 124 us; the launch traced here: 123 us
  starting transfers between devices  53.6 us (43%)
  waiting for transfers between devices  46.9 us (38%)
  Pallas kernels  9.49 us (8%)
  local copies, waits for them, and re-layouts  8.9 us (7%)
  other arithmetic  3.1 us (2%)
    ppermute x28, waiting for transfers between devices, send(): return lax.ppermute(value, AXES, pairs)  41.8 us
    ppermute x28, starting transfers between devices, send(): return lax.ppermute(value, AXES, pairs)  41.5 us
    all_to_all x2, starting transfers between devices, exchange(): return lax.all_to_all(tiles, axis, 0, 0, tiled=True)  12.1 us
    unnamed x25, local copies, waits for them, and re-layouts  7.24 us
    pallas_call x9, Pallas kernels, call(): pl.pallas_call(kernel, out_shape=outs, in_specs=in_specs, out_specs=jax.t...  5.19 us
    all_to_all x2, waiting for transfers between devices, exchange(): return lax.all_to_all(tiles, axis, 0, 0, tiled=True)  5.11 us
    pallas_call x1, Pallas kernels, body(): pl.pallas_call(recur_kernel, out_shape=[local(16, 256), shape(12, 2, 128,...  4.3 us
  transfers between devices with their start and end apart: 30, of which 18 were waited for; matrix products, arithmetic and copies ran while one was open for 3% of the time, Pallas kernels for 6%

profile of v3, /device:TPU:88, one launch (start us, length us, event | category | flops | bytes accessed | tf_op | source)
XLA Modules:
  0.0 122.9 jit_solution(1098480316994522411)
XLA Ops:
  0.6 0.8 copy.15.gain
  1.4 0.8 copy-done.6
  2.2 0.8 copy-done.7
  2.9 0.8 copy-done.8
  3.7 0.8 copy-done.9
  4.5 1.6 %collective-permute-start.2 = (bf16[64,1024]{1,0:T(8,128)(2,1)S(1)}, bf16[64,1024]{1,0:T(8,128)(2,1)S(1)}, u32[]{:S(2)}, u32[]{:S(2)}) collective-permute-start(bf16[64,1024]{1,0:T(8,128)(2,1)S(1)} %shard_map.141.w0), channel_id=1, source_target_pairs={{0,8},{1,9},{2,10},{3,11},{4,12},{5,13},{6,14},{7,15},{8,16},{9,17... | collective-permute-start | bytes 393224 | tf_op jit(solution)/shard_map/ppermute | solution.py:29
  6.1 2.7 %collective-permute-start.1 = (bf16[64,1024]{1,0:T(8,128)(2,1)S(1)}, bf16[64,1024]{1,0:T(8,128)(2,1)S(1)}, u32[]{:S(2)}, u32[]{:S(2)}) collective-permute-start(bf16[64,1024]{1,0:T(8,128)(2,1)S(1)} %shard_map.141.w0), channel_id=1, source_target_pairs={{0,16},{1,17},{2,18},{3,19},{4,20},{5,21},{6,22},{7,23},{8,24},{9,... | collective-permute-start | bytes 393224 | tf_op jit(solution)/shard_map/ppermute | solution.py:29
  8.8 1.4 %collective-permute-start = (bf16[64,1024]{1,0:T(8,128)(2,1)S(1)}, bf16[64,1024]{1,0:T(8,128)(2,1)S(1)}, u32[]{:S(2)}, u32[]{:S(2)}) collective-permute-start(bf16[64,1024]{1,0:T(8,128)(2,1)S(1)} %shard_map.141.w0), channel_id=1, source_target_pairs={{0,24},{1,25},{2,26},{3,27},{4,28},{5,29},{6,30},{7,31},{8,0},{9,1... | collective-permute-start | bytes 393224 | tf_op jit(solution)/shard_map/ppermute | solution.py:29
  11.0 1.0 multiply_convert_fusion
  12.0 0.9 maximum_maximum_fusion.rest_0_
  12.9 2.0 %collective-permute-start.10 = (bf16[144,1024]{1,0:T(8,128)(2,1)S(1)}, bf16[144,1024]{1,0:T(8,128)(2,1)S(1)}, u32[]{:S(2)}, u32[]{:S(2)}) collective-permute-start(bf16[144,1024]{1,0:T(8,128)(2,1)S(1)} %maximum_maximum_fusion.rest_0_), channel_id=1, source_target_pairs={{0,32},{1,33},{2,34},{3,35},{4,36},{5,37},{6,38},{7,39},{8,40},{9,... | collective-permute-start | bytes 884744 | tf_op jit(solution)/shard_map/ppermute | solution.py:29
  16.4 4.9 %all-to-all-start = ((bf16[32,8,128]{2,1,0:T(8,128)(2,1)}), bf16[32,8,128]{2,1,0:T(8,128)(2,1)S(1)}, u32[]{:S(2)}, u32[]{:S(2)}) async-start(bf16[32,8,128]{2,1,0:T(8,128)(2,1)} %shard_map.140), calls=%async_computation | async-start | bytes 131072 | tf_op jit(solution)/shard_map/all_to_all | solution.py:53
  21.8 5.1 %all-to-all-done.tok = bf16[32,8,128]{2,1,0:T(8,128)(2,1)S(1)} async-done(((bf16[32,8,128]{2,1,0:T(8,128)(2,1)}), bf16[32,8,128]{2,1,0:T(8,128)(2,1)S(1)}, u32[]{:S(2)}, u32[]{:S(2)}) %all-to-all-start) | async-done | bytes 65568 | tf_op jit(solution)/shard_map/all_to_all | solution.py:53
  27.0 1.9 %shard_map.142 = bf16[8,16,1024]{2,1,0:T(8,128)(2,1)} custom-call(s32[4]{0:T(128)} %and_select_fusion.4.x_at, bf16[32,8,128]{2,1,0:T(8,128)(2,1)S(1)} %all-to-all-done.tok, bf16[64,1024]{1,0:T(8,128)(2,1)S(1)} %shard_map.141.w0, bf16[64,1024]{1,0:T(8,128)(2,1)S(1)} %collective-permute-done.w1, bf16[64,1024]{1,0:T(8,128)(2,1)S(1)} %collective-permute-done.1.w2, ...), custom_call_target="tpu_custom_call" | custom-call | tf_op jit(solution)/shard_map/pallas_call | solution.py:103
  28.8 7.2 %all-to-all-start.1 = ((bf16[8,16,1024]{2,1,0:T(8,128)(2,1)}), bf16[8,16,1024]{2,1,0:T(8,128)(2,1)S(1)}, u32[]{:S(2)}, u32[]{:S(2)}) async-start(bf16[8,16,1024]{2,1,0:T(8,128)(2,1)} %shard_map.142), calls=%async_computation.1 | async-start | bytes 524288 | tf_op jit(solution)/shard_map/all_to_all | solution.py:53
  36.6 1.5 %collective-permute-start.11 = (bf16[144,1024]{1,0:T(8,128)(2,1)S(1)}, bf16[144,1024]{1,0:T(8,128)(2,1)S(1)}, u32[]{:S(2)}, u32[]{:S(2)}) collective-permute-start(bf16[144,1024]{1,0:T(8,128)(2,1)S(1)} %collective-permute-done.10.rest_7_), channel_id=1, source_target_pairs={{0,32},{1,33},{2,34},{3,35},{4,36},{5,37},{6,38},{7,39},{8,40},{9,... | collective-permute-start | bytes 884744 | tf_op jit(solution)/shard_map/ppermute | solution.py:29
  38.1 12.0 %collective-permute-done.6.rest_1_ = bf16[144,1024]{1,0:T(8,128)(2,1)S(1)} collective-permute-done((bf16[144,1024]{1,0:T(8,128)(2,1)S(1)}, bf16[144,1024]{1,0:T(8,128)(2,1)S(1)}, u32[]{:S(2)}, u32[]{:S(2)}) %collective-permute-start.6) | collective-permute-done | bytes 294944 | tf_op jit(solution)/shard_map/ppermute | solution.py:29
  50.6 7.0 %collective-permute-start.13 = (bf16[48,64]{1,0:T(8,128)(2,1)S(1)}, bf16[48,64]{1,0:T(8,128)(2,1)S(1)}, u32[]{:S(2)}, u32[]{:S(2)}) collective-permute-start(bf16[48,64]{1,0:T(8,128)(2,1)S(1)} %copy-done.11), channel_id=1, source_target_pairs={{0,0},{1,32},{2,64},{3,96},{4,128},{5,160},{6,192},{7,224},{8,8},{... | collective-permute-start | bytes 18440 | tf_op jit(solution)/shard_map/ppermute | solution.py:29
  57.8 4.3 %shard_map.143 = (bf16[16,256]{1,0:T(8,128)(2,1)S(1)}, f32[12,2,128,128]{3,2,1,0:T(8,128)}) custom-call(s32[1]{0:T(128)} %bitcast.1.place, bf16[8,16,1024]{2,1,0:T(8,128)(2,1)S(1)} %all-to-all-done.1.msg, f32[1,256]{1,0:T(1,128)} %bitcast.8, f32[2,128]{1,0:T(2,128)} %gain.1, f32[12,2,128,128]{3,2,1,0:T(8,128)} %state_hbm.1), custom_call_target="tpu_custom_call" | custom-call | tf_op jit(solution)/shard_map/pallas_call | solution.py:261
  62.1 2.0 %collective-permute-start.8 = (bf16[144,1024]{1,0:T(8,128)(2,1)S(1)}, bf16[144,1024]{1,0:T(8,128)(2,1)S(1)}, u32[]{:S(2)}, u32[]{:S(2)}) collective-permute-start(bf16[144,1024]{1,0:T(8,128)(2,1)S(1)} %collective-permute-done.7.rest_2_), channel_id=1, source_target_pairs={{0,224},{1,225},{2,226},{3,227},{4,228},{5,229},{6,230},{7,231},{8... | collective-permute-start | bytes 884744 | tf_op jit(solution)/shard_map/ppermute | solution.py:29
  65.0 2.0 %collective-permute-start.4 = (bf16[16,256]{1,0:T(8,128)(2,1)S(1)}, bf16[16,256]{1,0:T(8,128)(2,1)S(1)}, u32[]{:S(2)}, u32[]{:S(2)}) collective-permute-start(bf16[16,256]{1,0:T(8,128)(2,1)S(1)} %get-tuple-element.16.m0), channel_id=1, source_target_pairs={{0,16},{1,17},{2,18},{3,19},{4,20},{5,21},{6,22},{7,23},{8,24},{9,... | collective-permute-start | bytes 24584 | tf_op jit(solution)/shard_map/ppermute | solution.py:29
  67.2 1.1 collective-permute-start.3
  68.4 0.8 collective-permute-done.5.m3
  69.2 0.9 collective-permute-done.4.m2
  70.9 1.8 %collective-permute-done.8.rest_3_ = bf16[144,1024]{1,0:T(8,128)(2,1)S(1)} collective-permute-done((bf16[144,1024]{1,0:T(8,128)(2,1)S(1)}, bf16[144,1024]{1,0:T(8,128)(2,1)S(1)}, u32[]{:S(2)}, u32[]{:S(2)}) %collective-permute-start.8) | collective-permute-done | bytes 294944 | tf_op jit(solution)/shard_map/ppermute | solution.py:29
  72.6 0.9 shard_map.144.a
  73.5 3.0 %collective-permute-start.18 = (bf16[64,1024]{1,0:T(8,128)(2,1)S(1)}, bf16[64,1024]{1,0:T(8,128)(2,1)S(1)}, u32[]{:S(2)}, u32[]{:S(2)}) collective-permute-start(bf16[64,1024]{1,0:T(8,128)(2,1)S(1)} %slice.32), channel_id=1, source_target_pairs={{0,32},{1,33},{2,34},{3,35},{4,36},{5,37},{6,38},{7,39},{8,40},{9,... | collective-permute-start | bytes 393224 | tf_op jit(solution)/shard_map/ppermute | solution.py:29
  76.5 1.2 collective-permute-done.14.b
  77.8 3.1 %collective-permute-start.17 = (bf16[48,512]{1,0:T(8,128)(2,1)S(1)}, bf16[48,512]{1,0:T(8,128)(2,1)S(1)}, u32[]{:S(2)}, u32[]{:S(2)}) collective-permute-start(bf16[48,512]{1,0:T(8,128)(2,1)S(1)} %shard_map.145.s0), channel_id=1, source_target_pairs={{0,6},{1,7},{2,0},{3,1},{4,2},{5,3},{6,4},{7,5},{8,14},{9,15},{10,... | collective-permute-start | bytes 147464 | tf_op jit(solution)/shard_map/ppermute | solution.py:29
  81.1 1.9 %collective-permute-start.15 = (bf16[48,512]{1,0:T(8,128)(2,1)S(1)}, bf16[48,512]{1,0:T(8,128)(2,1)S(1)}, u32[]{:S(2)}, u32[]{:S(2)}) collective-permute-start(bf16[48,512]{1,0:T(8,128)(2,1)S(1)} %shard_map.145.s0), channel_id=1, source_target_pairs={{0,4},{1,5},{2,6},{3,7},{4,0},{5,1},{6,2},{7,3},{8,12},{9,13},{10,... | collective-permute-start | bytes 147464 | tf_op jit(solution)/shard_map/ppermute | solution.py:29
  83.2 1.8 %collective-permute-done.16.s2 = bf16[48,512]{1,0:T(8,128)(2,1)S(1)} collective-permute-done((bf16[48,512]{1,0:T(8,128)(2,1)S(1)}, bf16[48,512]{1,0:T(8,128)(2,1)S(1)}, u32[]{:S(2)}, u32[]{:S(2)}) %collective-permute-start.16) | collective-permute-done | bytes 49184 | tf_op jit(solution)/shard_map/ppermute | solution.py:29
  85.0 1.7 %collective-permute-done.15.s1 = bf16[48,512]{1,0:T(8,128)(2,1)S(1)} collective-permute-done((bf16[48,512]{1,0:T(8,128)(2,1)S(1)}, bf16[48,512]{1,0:T(8,128)(2,1)S(1)}, u32[]{:S(2)}, u32[]{:S(2)}) %collective-permute-start.15) | collective-permute-done | bytes 49184 | tf_op jit(solution)/shard_map/ppermute | solution.py:29
  86.7 1.0 copy-done.1
  87.7 1.0 copy-done.3
  88.6 1.0 copy-done.5
  89.9 1.2 collective-permute-start.21
  91.1 0.9 collective-permute-start.20
  92.0 1.2 %collective-permute-start.19 = (bf16[48,1152]{1,0:T(8,128)(2,1)S(1)}, bf16[48,1152]{1,0:T(8,128)(2,1)S(1)}, u32[]{:S(2)}, u32[]{:S(2)}) collective-permute-start(bf16[48,1152]{1,0:T(8,128)(2,1)S(1)} %get-tuple-element.21.h0), channel_id=1, source_target_pairs={{0,16},{1,17},{2,18},{3,19},{4,20},{5,21},{6,22},{7,23},{8,24},{9,... | collective-permute-start | bytes 331784 | tf_op jit(solution)/shard_map/ppermute | solution.py:29
  93.8 1.9 %collective-permute-done.21.h3 = bf16[48,1152]{1,0:T(8,128)(2,1)S(1)} collective-permute-done((bf16[48,1152]{1,0:T(8,128)(2,1)S(1)}, bf16[48,1152]{1,0:T(8,128)(2,1)S(1)}, u32[]{:S(2)}, u32[]{:S(2)}) %collective-permute-start.21) | collective-permute-done | bytes 110624 | tf_op jit(solution)/shard_map/ppermute | solution.py:29
  95.7 1.4 %collective-permute-done.20.h2 = bf16[48,1152]{1,0:T(8,128)(2,1)S(1)} collective-permute-done((bf16[48,1152]{1,0:T(8,128)(2,1)S(1)}, bf16[48,1152]{1,0:T(8,128)(2,1)S(1)}, u32[]{:S(2)}, u32[]{:S(2)}) %collective-permute-start.20) | collective-permute-done | bytes 110624 | tf_op jit(solution)/shard_map/ppermute | solution.py:29
  97.1 1.2 collective-permute-done.19.h1
  98.3 1.2 shard_map.147
  99.6 1.2 collective-permute-done.23.came
  100.8 2.1 %collective-permute-start.24 = (bf16[48,64]{1,0:T(8,128)(2,1)S(1)}, bf16[48,64]{1,0:T(8,128)(2,1)S(1)}, u32[]{:S(2)}, u32[]{:S(2)}) collective-permute-start(bf16[48,64]{1,0:T(8,128)(2,1)S(1)} %get-tuple-element.26), channel_id=1, source_target_pairs={{0,4},{1,5},{2,6},{3,7},{4,0},{5,1},{6,2},{7,3},{8,12},{9,13},{10,... | collective-permute-start | bytes 18440 | tf_op jit(solution)/shard_map/ppermute | solution.py:29
  103.0 2.4 %collective-permute-start.25 = (bf16[48,64]{1,0:T(8,128)(2,1)S(1)}, bf16[48,64]{1,0:T(8,128)(2,1)S(1)}, u32[]{:S(2)}, u32[]{:S(2)}) collective-permute-start(bf16[48,64]{1,0:T(8,128)(2,1)S(1)} %get-tuple-element.27), channel_id=1, source_target_pairs={{0,2},{1,3},{2,4},{3,5},{4,6},{5,7},{6,0},{7,1},{8,10},{9,11},{10,... | collective-permute-start | bytes 18440 | tf_op jit(solution)/shard_map/ppermute | solution.py:29
  106.8 3.5 %collective-permute-done.26.p3 = bf16[48,64]{1,0:T(8,128)(2,1)S(1)} collective-permute-done((bf16[48,64]{1,0:T(8,128)(2,1)S(1)}, bf16[48,64]{1,0:T(8,128)(2,1)S(1)}, u32[]{:S(2)}, u32[]{:S(2)}) %collective-permute-start.26) | collective-permute-done | bytes 6176 | tf_op jit(solution)/shard_map/ppermute | solution.py:29
  110.4 1.9 %collective-permute-start.27 = (bf16[48,64]{1,0:T(8,128)(2,1)S(1)}, bf16[48,64]{1,0:T(8,128)(2,1)S(1)}, u32[]{:S(2)}, u32[]{:S(2)}) collective-permute-start(bf16[48,64]{1,0:T(8,128)(2,1)S(1)} %shard_map.149), channel_id=1, source_target_pairs={{0,0},{1,32},{2,64},{3,96},{4,128},{5,160},{6,192},{7,224},{8,8},{... | collective-permute-start | bytes 18440 | tf_op jit(solution)/shard_map/ppermute | solution.py:29
  112.3 10.0 %collective-permute-done.27 = bf16[48,64]{1,0:T(8,128)(2,1)S(1)} collective-permute-done((bf16[48,64]{1,0:T(8,128)(2,1)S(1)}, bf16[48,64]{1,0:T(8,128)(2,1)S(1)}, u32[]{:S(2)}, u32[]{:S(2)}) %collective-permute-start.27) | collective-permute-done | bytes 6176 | tf_op jit(solution)/shard_map/ppermute | solution.py:29
  (61 shorter events, 9.5 us)
Async XLA Ops:
  0.6 50.0 %copy-start.11 = (bf16[48,64]{1,0:T(8,128)(2,1)S(1)}, bf16[48,64]{1,0:T(8,128)(2,1)}, u32[]{:S(2)}) copy-start(bf16[48,64]{1,0:T(8,128)(2,1)} %tok.1) | copy-start | bytes 18436
  1.4 0.8 copy-start.6
  2.2 0.8 copy-start.7
  2.9 0.8 copy-start.8
  3.7 0.8 copy-start.9
  4.5 22.4 %collective-permute-start.2 = (bf16[64,1024]{1,0:T(8,128)(2,1)S(1)}, bf16[64,1024]{1,0:T(8,128)(2,1)S(1)}, u32[]{:S(2)}, u32[]{:S(2)}) collective-permute-start(bf16[64,1024]{1,0:T(8,128)(2,1)S(1)} %shard_map.141.w0), channel_id=1, source_target_pairs={{0,8},{1,9},{2,10},{3,11},{4,12},{5,13},{6,14},{7,15},{8,16},{9,17... | collective-permute-start | bytes 393224 | tf_op jit(solution)/shard_map/ppermute | solution.py:29
  6.1 20.8 %collective-permute-start.1 = (bf16[64,1024]{1,0:T(8,128)(2,1)S(1)}, bf16[64,1024]{1,0:T(8,128)(2,1)S(1)}, u32[]{:S(2)}, u32[]{:S(2)}) collective-permute-start(bf16[64,1024]{1,0:T(8,128)(2,1)S(1)} %shard_map.141.w0), channel_id=1, source_target_pairs={{0,16},{1,17},{2,18},{3,19},{4,20},{5,21},{6,22},{7,23},{8,24},{9,... | collective-permute-start | bytes 393224 | tf_op jit(solution)/shard_map/ppermute | solution.py:29
  8.8 18.1 %collective-permute-start = (bf16[64,1024]{1,0:T(8,128)(2,1)S(1)}, bf16[64,1024]{1,0:T(8,128)(2,1)S(1)}, u32[]{:S(2)}, u32[]{:S(2)}) collective-permute-start(bf16[64,1024]{1,0:T(8,128)(2,1)S(1)} %shard_map.141.w0), channel_id=1, source_target_pairs={{0,24},{1,25},{2,26},{3,27},{4,28},{5,29},{6,30},{7,31},{8,0},{9,1... | collective-permute-start | bytes 393224 | tf_op jit(solution)/shard_map/ppermute | solution.py:29
  12.9 23.7 %collective-permute-start.10 = (bf16[144,1024]{1,0:T(8,128)(2,1)S(1)}, bf16[144,1024]{1,0:T(8,128)(2,1)S(1)}, u32[]{:S(2)}, u32[]{:S(2)}) collective-permute-start(bf16[144,1024]{1,0:T(8,128)(2,1)S(1)} %maximum_maximum_fusion.rest_0_), channel_id=1, source_target_pairs={{0,32},{1,33},{2,34},{3,35},{4,36},{5,37},{6,38},{7,39},{8,40},{9,... | collective-permute-start | bytes 884744 | tf_op jit(solution)/shard_map/ppermute | solution.py:29
  14.9 0.7 copy-start.10
  16.4 10.6 %all-to-all-start = ((bf16[32,8,128]{2,1,0:T(8,128)(2,1)}), bf16[32,8,128]{2,1,0:T(8,128)(2,1)S(1)}, u32[]{:S(2)}, u32[]{:S(2)}) async-start(bf16[32,8,128]{2,1,0:T(8,128)(2,1)} %shard_map.140), calls=%async_computation | async-start | bytes 131072 | tf_op jit(solution)/shard_map/all_to_all | solution.py:53
  28.8 28.8 %all-to-all-start.1 = ((bf16[8,16,1024]{2,1,0:T(8,128)(2,1)}), bf16[8,16,1024]{2,1,0:T(8,128)(2,1)S(1)}, u32[]{:S(2)}, u32[]{:S(2)}) async-start(bf16[8,16,1024]{2,1,0:T(8,128)(2,1)} %shard_map.142), calls=%async_computation.1 | async-start | bytes 524288 | tf_op jit(solution)/shard_map/all_to_all | solution.py:53
  36.0 14.0 %collective-permute-start.6 = (bf16[144,1024]{1,0:T(8,128)(2,1)S(1)}, bf16[144,1024]{1,0:T(8,128)(2,1)S(1)}, u32[]{:S(2)}, u32[]{:S(2)}) collective-permute-start(bf16[144,1024]{1,0:T(8,128)(2,1)S(1)} %maximum_maximum_fusion.rest_0_), channel_id=1, source_target_pairs={{0,224},{1,225},{2,226},{3,227},{4,228},{5,229},{6,230},{7,231},{8... | collective-permute-start | bytes 884744 | tf_op jit(solution)/shard_map/ppermute | solution.py:29
  36.6 21.0 %collective-permute-start.11 = (bf16[144,1024]{1,0:T(8,128)(2,1)S(1)}, bf16[144,1024]{1,0:T(8,128)(2,1)S(1)}, u32[]{:S(2)}, u32[]{:S(2)}) collective-permute-start(bf16[144,1024]{1,0:T(8,128)(2,1)S(1)} %collective-permute-done.10.rest_7_), channel_id=1, source_target_pairs={{0,32},{1,33},{2,34},{3,35},{4,36},{5,37},{6,38},{7,39},{8,40},{9,... | collective-permute-start | bytes 884744 | tf_op jit(solution)/shard_map/ppermute | solution.py:29
  50.0 23.5 %copy-start.2 = (bf16[144,1024]{1,0:T(8,128)(2,1)}, bf16[144,1024]{1,0:T(8,128)(2,1)S(1)}, u32[]{:S(2)}) copy-start(bf16[144,1024]{1,0:T(8,128)(2,1)S(1)} %collective-permute-done.6.rest_1_) | copy-start | bytes 884740
  50.0 12.1 %collective-permute-start.7 = (bf16[144,1024]{1,0:T(8,128)(2,1)S(1)}, bf16[144,1024]{1,0:T(8,128)(2,1)S(1)}, u32[]{:S(2)}, u32[]{:S(2)}) collective-permute-start(bf16[144,1024]{1,0:T(8,128)(2,1)S(1)} %collective-permute-done.6.rest_1_), channel_id=1, source_target_pairs={{0,224},{1,225},{2,226},{3,227},{4,228},{5,229},{6,230},{7,231},{8... | collective-permute-start | bytes 884744 | tf_op jit(solution)/shard_map/ppermute | solution.py:29
  50.6 13.5 %collective-permute-start.13 = (bf16[48,64]{1,0:T(8,128)(2,1)S(1)}, bf16[48,64]{1,0:T(8,128)(2,1)S(1)}, u32[]{:S(2)}, u32[]{:S(2)}) collective-permute-start(bf16[48,64]{1,0:T(8,128)(2,1)S(1)} %copy-done.11), channel_id=1, source_target_pairs={{0,0},{1,32},{2,64},{3,96},{4,128},{5,160},{6,192},{7,224},{8,8},{... | collective-permute-start | bytes 18440 | tf_op jit(solution)/shard_map/ppermute | solution.py:29
  57.6 15.9 %copy-start.4 = (bf16[144,1024]{1,0:T(8,128)(2,1)}, bf16[144,1024]{1,0:T(8,128)(2,1)S(1)}, u32[]{:S(2)}) copy-start(bf16[144,1024]{1,0:T(8,128)(2,1)S(1)} %collective-permute-done.11.rest_6_) | copy-start | bytes 884740
  57.6 9.6 %collective-permute-start.12 = (bf16[144,1024]{1,0:T(8,128)(2,1)S(1)}, bf16[144,1024]{1,0:T(8,128)(2,1)S(1)}, u32[]{:S(2)}, u32[]{:S(2)}) collective-permute-start(bf16[144,1024]{1,0:T(8,128)(2,1)S(1)} %collective-permute-done.11.rest_6_), channel_id=1, source_target_pairs={{0,32},{1,33},{2,34},{3,35},{4,36},{5,37},{6,38},{7,39},{8,40},{9,... | collective-permute-start | bytes 884744 | tf_op jit(solution)/shard_map/ppermute | solution.py:29
  57.7 10.7 %collective-permute-start.9 = (bf16[16,1024]{1,0:T(8,128)(2,1)S(1)}, bf16[16,1024]{1,0:T(8,128)(2,1)S(1)}, u32[]{:S(2)}, u32[]{:S(2)}) collective-permute-start(bf16[16,1024]{1,0:T(8,128)(2,1)S(1)} %pad_maximum_fusion), channel_id=1, source_target_pairs={{0,128},{1,129},{2,130},{3,131},{4,132},{5,133},{6,134},{7,135},{8... | collective-permute-start | bytes 98312 | tf_op jit(solution)/shard_map/ppermute | solution.py:29
  62.1 10.5 %collective-permute-start.8 = (bf16[144,1024]{1,0:T(8,128)(2,1)S(1)}, bf16[144,1024]{1,0:T(8,128)(2,1)S(1)}, u32[]{:S(2)}, u32[]{:S(2)}) collective-permute-start(bf16[144,1024]{1,0:T(8,128)(2,1)S(1)} %collective-permute-done.7.rest_2_), channel_id=1, source_target_pairs={{0,224},{1,225},{2,226},{3,227},{4,228},{5,229},{6,230},{7,231},{8... | collective-permute-start | bytes 884744 | tf_op jit(solution)/shard_map/ppermute | solution.py:29
  64.3 4.9 %collective-permute-start.5 = (bf16[16,256]{1,0:T(8,128)(2,1)S(1)}, bf16[16,256]{1,0:T(8,128)(2,1)S(1)}, u32[]{:S(2)}, u32[]{:S(2)}) collective-permute-start(bf16[16,256]{1,0:T(8,128)(2,1)S(1)} %get-tuple-element.16.m0), channel_id=1, source_target_pairs={{0,8},{1,9},{2,10},{3,11},{4,12},{5,13},{6,14},{7,15},{8,16},{9,17... | collective-permute-start | bytes 24584 | tf_op jit(solution)/shard_map/ppermute | solution.py:29
  65.0 5.2 %collective-permute-start.4 = (bf16[16,256]{1,0:T(8,128)(2,1)S(1)}, bf16[16,256]{1,0:T(8,128)(2,1)S(1)}, u32[]{:S(2)}, u32[]{:S(2)}) collective-permute-start(bf16[16,256]{1,0:T(8,128)(2,1)S(1)} %get-tuple-element.16.m0), channel_id=1, source_target_pairs={{0,16},{1,17},{2,18},{3,19},{4,20},{5,21},{6,22},{7,23},{8,24},{9,... | collective-permute-start | bytes 24584 | tf_op jit(solution)/shard_map/ppermute | solution.py:29
  67.2 3.7 %collective-permute-start.3 = (bf16[16,256]{1,0:T(8,128)(2,1)S(1)}, bf16[16,256]{1,0:T(8,128)(2,1)S(1)}, u32[]{:S(2)}, u32[]{:S(2)}) collective-permute-start(bf16[16,256]{1,0:T(8,128)(2,1)S(1)} %get-tuple-element.16.m0), channel_id=1, source_target_pairs={{0,24},{1,25},{2,26},{3,27},{4,28},{5,29},{6,30},{7,31},{8,0},{9,1... | collective-permute-start | bytes 24584 | tf_op jit(solution)/shard_map/ppermute | solution.py:29
  72.6 10.4 %copy-start = (bf16[144,1024]{1,0:T(8,128)(2,1)}, bf16[144,1024]{1,0:T(8,128)(2,1)S(1)}, u32[]{:S(2)}) copy-start(bf16[144,1024]{1,0:T(8,128)(2,1)S(1)} %collective-permute-done.8.rest_3_) | copy-start | bytes 884740
  73.5 13.2 %collective-permute-start.18 = (bf16[64,1024]{1,0:T(8,128)(2,1)S(1)}, bf16[64,1024]{1,0:T(8,128)(2,1)S(1)}, u32[]{:S(2)}, u32[]{:S(2)}) collective-permute-start(bf16[64,1024]{1,0:T(8,128)(2,1)S(1)} %slice.32), channel_id=1, source_target_pairs={{0,32},{1,33},{2,34},{3,35},{4,36},{5,37},{6,38},{7,39},{8,40},{9,... | collective-permute-start | bytes 393224 | tf_op jit(solution)/shard_map/ppermute | solution.py:29
  76.5 1.2 %collective-permute-start.14 = (bf16[48,512]{1,0:T(8,128)(2,1)S(1)}, bf16[48,512]{1,0:T(8,128)(2,1)S(1)}, u32[]{:S(2)}, u32[]{:S(2)}) collective-permute-start(bf16[48,512]{1,0:T(8,128)(2,1)S(1)} %shard_map.144.a), channel_id=1, source_target_pairs={{0,1},{1,0},{2,3},{3,2},{4,5},{5,4},{6,7},{7,6},{8,9},{9,8},{10,11... | collective-permute-start | bytes 147464 | tf_op jit(solution)/shard_map/ppermute | solution.py:29
  77.8 5.4 %collective-permute-start.17 = (bf16[48,512]{1,0:T(8,128)(2,1)S(1)}, bf16[48,512]{1,0:T(8,128)(2,1)S(1)}, u32[]{:S(2)}, u32[]{:S(2)}) collective-permute-start(bf16[48,512]{1,0:T(8,128)(2,1)S(1)} %shard_map.145.s0), channel_id=1, source_target_pairs={{0,6},{1,7},{2,0},{3,1},{4,2},{5,3},{6,4},{7,5},{8,14},{9,15},{10,... | collective-permute-start | bytes 147464 | tf_op jit(solution)/shard_map/ppermute | solution.py:29
  80.9 4.1 %collective-permute-start.16 = (bf16[48,512]{1,0:T(8,128)(2,1)S(1)}, bf16[48,512]{1,0:T(8,128)(2,1)S(1)}, u32[]{:S(2)}, u32[]{:S(2)}) collective-permute-start(bf16[48,512]{1,0:T(8,128)(2,1)S(1)} %shard_map.145.s0), channel_id=1, source_target_pairs={{0,2},{1,3},{2,4},{3,5},{4,6},{5,7},{6,0},{7,1},{8,10},{9,11},{10,... | collective-permute-start | bytes 147464 | tf_op jit(solution)/shard_map/ppermute | solution.py:29
  81.1 5.6 %collective-permute-start.15 = (bf16[48,512]{1,0:T(8,128)(2,1)S(1)}, bf16[48,512]{1,0:T(8,128)(2,1)S(1)}, u32[]{:S(2)}, u32[]{:S(2)}) collective-permute-start(bf16[48,512]{1,0:T(8,128)(2,1)S(1)} %shard_map.145.s0), channel_id=1, source_target_pairs={{0,4},{1,5},{2,6},{3,7},{4,0},{5,1},{6,2},{7,3},{8,12},{9,13},{10,... | collective-permute-start | bytes 147464 | tf_op jit(solution)/shard_map/ppermute | solution.py:29
  83.1 10.8 %collective-permute-start.22 = (bf16[64,1024]{1,0:T(8,128)(2,1)S(1)}, bf16[64,1024]{1,0:T(8,128)(2,1)S(1)}, u32[]{:S(2)}, u32[]{:S(2)}) collective-permute-start(bf16[64,1024]{1,0:T(8,128)(2,1)S(1)} %slice.33), channel_id=1, source_target_pairs={{0,224},{1,225},{2,226},{3,227},{4,228},{5,229},{6,230},{7,231},{8... | collective-permute-start | bytes 393224 | tf_op jit(solution)/shard_map/ppermute | solution.py:29
  86.7 1.0 copy-start.1
  87.7 1.0 copy-start.3
  88.6 1.0 copy-start.5
  89.9 5.8 %collective-permute-start.21 = (bf16[48,1152]{1,0:T(8,128)(2,1)S(1)}, bf16[48,1152]{1,0:T(8,128)(2,1)S(1)}, u32[]{:S(2)}, u32[]{:S(2)}) collective-permute-start(bf16[48,1152]{1,0:T(8,128)(2,1)S(1)} %get-tuple-element.21.h0), channel_id=1, source_target_pairs={{0,24},{1,25},{2,26},{3,27},{4,28},{5,29},{6,30},{7,31},{8,0},{9,1... | collective-permute-start | bytes 331784 | tf_op jit(solution)/shard_map/ppermute | solution.py:29
  91.1 6.0 %collective-permute-start.20 = (bf16[48,1152]{1,0:T(8,128)(2,1)S(1)}, bf16[48,1152]{1,0:T(8,128)(2,1)S(1)}, u32[]{:S(2)}, u32[]{:S(2)}) collective-permute-start(bf16[48,1152]{1,0:T(8,128)(2,1)S(1)} %get-tuple-element.21.h0), channel_id=1, source_target_pairs={{0,8},{1,9},{2,10},{3,11},{4,12},{5,13},{6,14},{7,15},{8,16},{9,17... | collective-permute-start | bytes 331784 | tf_op jit(solution)/shard_map/ppermute | solution.py:29
  92.0 6.3 %collective-permute-start.19 = (bf16[48,1152]{1,0:T(8,128)(2,1)S(1)}, bf16[48,1152]{1,0:T(8,128)(2,1)S(1)}, u32[]{:S(2)}, u32[]{:S(2)}) collective-permute-start(bf16[48,1152]{1,0:T(8,128)(2,1)S(1)} %get-tuple-element.21.h0), channel_id=1, source_target_pairs={{0,16},{1,17},{2,18},{3,19},{4,20},{5,21},{6,22},{7,23},{8,24},{9,... | collective-permute-start | bytes 331784 | tf_op jit(solution)/shard_map/ppermute | solution.py:29
  99.5 1.3 %collective-permute-start.23 = (bf16[4,48,64]{2,1,0:T(8,128)(2,1)S(1)}, bf16[4,48,64]{2,1,0:T(8,128)(2,1)S(1)}, u32[]{:S(2)}, u32[]{:S(2)}) collective-permute-start(bf16[4,48,64]{2,1,0:T(8,128)(2,1)S(1)} %get-tuple-element.24), channel_id=1, source_target_pairs={{0,1},{1,0},{2,3},{3,2},{4,5},{5,4},{6,7},{7,6},{8,9},{9,8},{10,11... | collective-permute-start | bytes 73736 | tf_op jit(solution)/shard_map/ppermute | solution.py:29
  100.8 5.3 %collective-permute-start.24 = (bf16[48,64]{1,0:T(8,128)(2,1)S(1)}, bf16[48,64]{1,0:T(8,128)(2,1)S(1)}, u32[]{:S(2)}, u32[]{:S(2)}) collective-permute-start(bf16[48,64]{1,0:T(8,128)(2,1)S(1)} %get-tuple-element.26), channel_id=1, source_target_pairs={{0,4},{1,5},{2,6},{3,7},{4,0},{5,1},{6,2},{7,3},{8,12},{9,13},{10,... | collective-permute-start | bytes 18440 | tf_op jit(solution)/shard_map/ppermute | solution.py:29
  103.0 3.8 %collective-permute-start.25 = (bf16[48,64]{1,0:T(8,128)(2,1)S(1)}, bf16[48,64]{1,0:T(8,128)(2,1)S(1)}, u32[]{:S(2)}, u32[]{:S(2)}) collective-permute-start(bf16[48,64]{1,0:T(8,128)(2,1)S(1)} %get-tuple-element.27), channel_id=1, source_target_pairs={{0,2},{1,3},{2,4},{3,5},{4,6},{5,7},{6,0},{7,1},{8,10},{9,11},{10,... | collective-permute-start | bytes 18440 | tf_op jit(solution)/shard_map/ppermute | solution.py:29
  105.4 4.9 %collective-permute-start.26 = (bf16[48,64]{1,0:T(8,128)(2,1)S(1)}, bf16[48,64]{1,0:T(8,128)(2,1)S(1)}, u32[]{:S(2)}, u32[]{:S(2)}) collective-permute-start(bf16[48,64]{1,0:T(8,128)(2,1)S(1)} %get-tuple-element.28), channel_id=1, source_target_pairs={{0,6},{1,7},{2,0},{3,1},{4,2},{5,3},{6,4},{7,5},{8,14},{9,15},{10,... | collective-permute-start | bytes 18440 | tf_op jit(solution)/shard_map/ppermute | solution.py:29
  110.4 11.9 %collective-permute-start.27 = (bf16[48,64]{1,0:T(8,128)(2,1)S(1)}, bf16[48,64]{1,0:T(8,128)(2,1)S(1)}, u32[]{:S(2)}, u32[]{:S(2)}) collective-permute-start(bf16[48,64]{1,0:T(8,128)(2,1)S(1)} %shard_map.149), channel_id=1, source_target_pairs={{0,0},{1,32},{2,64},{3,96},{4,128},{5,160},{6,192},{7,224},{8,8},{... | collective-permute-start | bytes 18440 | tf_op jit(solution)/shard_map/ppermute | solution.py:29
